TPU v7x, 128 devices: a whole 4x4x4 slice. The times are simulated.
128 devices in a mesh: ep: 64 (over z, y, x), tp: 2 (over core).
Axes of the slice: x: 4, y: 4, z: 4, core: 2. Of those that a mesh axis runs over, the one named last changes fastest.
Arguments:
- tokens: bfloat16 [1536, 2048], P('ep'), may hold values from -6 to 6
- norm_gain: bfloat16 [2048], replicated, may hold values from 0.099609375 to 1.8984375
- query_w: bfloat16 [2048, 1024], P(None, 'tp'), may hold values from -0.125 to 0.125
- key_w: bfloat16 [2048, 128], replicated, may hold values from -0.125 to 0.125
- value_w: bfloat16 [2048, 128], replicated, may hold values from -0.125 to 0.125
- forget_w: bfloat16 [2048, 16], replicated, may hold values from -0.125 to 0.125
- forget_bias: float32 [16], replicated, may hold values from 0 to 4
- query_gain: bfloat16 [64], replicated, may hold values from 0.099609375 to 1.8984375
- key_gain: bfloat16 [64], replicated, may hold values from 0.099609375 to 1.8984375
- cache_key: bfloat16 [1536, 2, 64, 1024], P('ep', 'tp'), may hold values from -6 to 6
- cache_value: bfloat16 [1536, 2, 64, 1024], P('ep', 'tp'), may hold values from -6 to 6
- cache_gate: float32 [1536, 16, 1024], P('ep', 'tp'), may hold values from -105 to 0, as said below
- cache_len: int32 [1536], P('ep'), may hold values from 256 to 1024
- out_w: bfloat16 [1024, 2048], P('tp'), may hold values from -0.1875 to 0.1875
- post_gain: bfloat16 [2048], replicated, may hold values from 0.099609375 to 1.8984375
- branch_gate: bfloat16 [2048], replicated, may hold values from -0.125 to 0.125
- dense_gate_w: bfloat16 [2048, 16384], P(None, ('ep', 'tp')), may hold values from -0.125 to 0.125
- dense_up_w: bfloat16 [2048, 16384], P(None, ('ep', 'tp')), may hold values from -1.3258252 to 1.3258252
- dense_down_w: bfloat16 [16384, 2048], P(('ep', 'tp')), may hold values from -0.046875 to 0.046875
- expert_choice: int32 [1536, 2], P('ep'), may hold values from 0 to 63, as said below
- route_weight: float32 [1536, 2], P('ep'), may hold values from 0.1 to 1
- expert_gate_w: bfloat16 [64, 2048, 1024], P('ep', None, 'tp'), may hold values from -0.125 to 0.125
- expert_up_w: bfloat16 [64, 2048, 1024], P('ep', None, 'tp'), may hold values from -0.125 to 0.125
- expert_down_w: bfloat16 [64, 1024, 2048], P('ep', 'tp'), may hold values from -0.1875 to 0.1875
Outputs:
- mixed_out: bfloat16 [1536, 2048], P('ep', 'tp')
- fresh_key: bfloat16 [1536, 2, 64], P('ep', 'tp')
- fresh_value: bfloat16 [1536, 2, 64], P('ep', 'tp')
- fresh_gate: float32 [1536, 16], P('ep', 'tp')
Inputs may be any that keep to these rules, and one draw needn't show every extreme that they name: `cache_gate`: Non-increasing along positions. `expert_choice`: experts 16 * g to 16 * g + 15 form group g. A token names 2 different experts of one group. Among the 24 tokens of one index of ep, those at even offsets all choose one group and the others choose other groups; no expert is named more than 2 times by them, and some expert exactly 2 times.
All inputs are finite; a program needn't handle non-finite values.
Results may differ from a plain program's by a relative error of at most 0.014.
Values may be sent and summed in bfloat16 or wider, within the bound.
No kernel may reach another device: no remote copies, remote signals or barrier semaphores. Data moves between devices by JAX's collectives and lax.ppermute only.
A program may use at most 128 MiB of HBM per device.

v0:
```python
import functools

import jax
import jax.numpy as jnp
from jax import lax
from jax.experimental import pallas as pl
from jax.experimental.pallas import tpu as pltpu
from jax.sharding import PartitionSpec as P


FF2 = 16384
LANES = 128
INFO = 128
SLOTS = 2
EPS = 1e-06
SWAP = [(0, 1), (1, 0)]
F32 = jnp.float32
BF16 = jnp.bfloat16


def class_of(e):
    return (e ^ (e // 2)) % 2


def swapped(array):
    return lax.ppermute(array, "tp", SWAP)


def iota(shape, dim):
    return lax.broadcasted_iota(jnp.int32, shape, dim)


def mm(a, b):
    return jnp.dot(a, b, preferred_element_type=F32)


def mm_t(a, b):
    return lax.dot_general(a, b, (((1,), (1,)), ((), ())), preferred_element_type=F32)


def silu(v):
    return v / (1.0 + jnp.exp(-v))


def params(limit=56):
    return pltpu.CompilerParams(vmem_limit_bytes=limit << 20)


def whole(shape):
    return pl.BlockSpec(shape, lambda *_: (0,) * len(shape))


def near_call(kernel, arrays, outs, scratch=(), limit=32):
    here = pl.BlockSpec(memory_space=pltpu.VMEM)
    many = isinstance(outs, list)
    return pl.pallas_call(
        kernel,
        in_specs=[here] * len(arrays),
        out_specs=[here] * len(outs) if many else here,
        out_shape=outs,
        scratch_shapes=list(scratch),
        compiler_params=params(limit),
    )(*arrays)


def kept(ref, dim, size, other=False):
    rank = lax.axis_index("tp")
    rank = 1 - rank if other else rank
    at = pl.ds(pl.multiple_of(rank * size, size), size)
    return ref[at, :] if dim == 0 else ref[:, at]


def laid_out(ref):
    rows = ref[...].astype(F32)
    return jnp.concatenate([rows[r : r + 1, :] for r in range(rows.shape[0])], axis=1)


def tiled(vector):
    return vector.reshape(-1, LANES)


def attend_kernel(
    len_ref, tok, ng, qw, kw, vw, fw, fb, qg, kg, key, val, gate, ow,
    partial, fk_out, fv_out, cur_out, q_scr, own_scr, lf_scr, fv_scr, heads_scr, *, block, steps,
):
    step = pl.program_id(0)
    count = tok.shape[0]
    heads = gate.shape[1]
    hd = key.shape[2]
    span = key.shape[3]
    rows = count * heads
    width = heads * hd
    scale = hd ** (-0.5)
    second = lax.axis_index("tp") == 1

    @pl.when(step == 0)
    def _():
        x = tok[...].astype(F32)
        ms = jnp.mean(x * x, axis=1, keepdims=True)
        normed = (x * lax.rsqrt(ms + EPS) * laid_out(ng)).astype(BF16)
        q = mm(normed, qw[...])
        k = mm(normed, kw[...])
        v = mm(normed, vw[...])
        k = jnp.where(second, k[:, hd:], k[:, :hd])
        v = jnp.where(second, v[:, hd:], v[:, :hd]).astype(BF16)
        k = k * lax.rsqrt(jnp.mean(k * k, axis=1, keepdims=True) + EPS) * kg[...].astype(F32)
        k = k.astype(BF16)
        fk_out[...] = k
        fv_out[...] = v
        spread = jnp.broadcast_to(q[:, None, :], (count, heads, width)).reshape(rows, width)
        mine = iota((rows, width), 1) // hd == iota((rows, width), 0) % heads
        spread = jnp.where(mine, spread, 0.0)
        msq = jnp.sum(spread * spread, axis=1, keepdims=True) / hd
        spread = spread * lax.rsqrt(msq + EPS)
        gain = jnp.concatenate([qg[...].astype(F32)] * heads, axis=1)
        spread = (spread * gain).astype(BF16)
        pick = (iota((width, hd), 0) % hd == iota((width, hd), 1)).astype(BF16)
        queries = mm(spread, pick)
        q_scr[...] = queries.astype(BF16)
        k_rows = jnp.broadcast_to(k.astype(F32)[:, None, :], (count, heads, hd)).reshape(rows, hd)
        own = jnp.sum(queries * k_rows, axis=1, keepdims=True) * scale
        own_scr[...] = jnp.broadcast_to(own, (rows, LANES))
        fv_scr[...] = jnp.broadcast_to(v.astype(F32)[:, None, :], (count, heads, hd)).reshape(rows, hd)
        local = jnp.where(second, fw[heads:, :].astype(F32), fw[:heads, :].astype(F32)).astype(BF16)
        bias = jnp.where(second, fb[:, heads:], fb[:, :heads])
        lf = jax.nn.log_sigmoid(mm_t(normed, local) + bias)
        lf = jnp.broadcast_to(lf[:, None, :], (count, heads, heads)).reshape(rows, heads)
        lf = jnp.where(iota((rows, heads), 1) == iota((rows, heads), 0) % heads, lf, 0.0)
        lf_scr[...] = jnp.broadcast_to(jnp.sum(lf, axis=1, keepdims=True), (rows, LANES))

    part = block * heads
    at = pl.ds(pl.multiple_of(step * part, part), part)
    queries = q_scr[at, :]
    scores = jnp.concatenate(
        [mm(queries[i * heads : (i + 1) * heads, :], key[i, 0]) for i in range(block)], axis=0
    )
    pos = iota((part, span), 1)
    length = jnp.concatenate(
        [jnp.full((heads, 1), len_ref[step * block + i], jnp.int32) for i in range(block)], axis=0
    )
    gates = gate[...].reshape(part, span)
    previous = jnp.sum(jnp.where(pos == length - 1, gates, 0.0), axis=1, keepdims=True)
    current = previous + lf_scr[at, :][:, :1]
    logits = jnp.where(pos < length, scores * scale + (current - gates), -jnp.inf)
    own = own_scr[at, :][:, :1]
    top = jnp.maximum(jnp.max(logits, axis=1, keepdims=True), own)
    weights = jnp.exp(logits - top)
    own_weight = jnp.exp(own - top)
    total = jnp.sum(weights, axis=1, keepdims=True) + own_weight
    probs = (weights / total).astype(BF16)
    own_prob = (own_weight / total).astype(BF16).astype(F32)
    mixed = jnp.concatenate(
        [mm_t(probs[i * heads : (i + 1) * heads, :], val[i, 0]) for i in range(block)], axis=0
    )
    mixed = mixed + own_prob * fv_scr[at, :]
    heads_scr[at, :] = mixed.astype(BF16).astype(F32)
    spot = iota((part, heads), 1) == iota((part, heads), 0) % heads
    cur = jnp.where(spot, current, 0.0).reshape(block, heads, heads)
    cur_out[pl.ds(pl.multiple_of(step * block, block), block), :] = jnp.sum(cur, axis=1)

    @pl.when(step == steps - 1)
    def _():
        pick = (iota((hd, width), 1) % hd == iota((hd, width), 0)).astype(BF16)
        wide = mm(heads_scr[...].astype(BF16), pick)
        mine = iota((rows, width), 1) // hd == iota((rows, width), 0) % heads
        wide = jnp.where(mine, wide, 0.0).reshape(count, heads, width)
        flat = jnp.sum(wide, axis=1).astype(BF16)
        partial[...] = mm(flat, ow[...]).astype(BF16)


def attend(lens, tok, ng, qw, kw, vw, fw, fb, qg, kg, key, val, gate, ow):
    count, heads, span = gate.shape
    hd = key.shape[2]
    width = tok.shape[1]
    block = 8
    steps = count // block
    rows = count * heads
    return pl.pallas_call(
        functools.partial(attend_kernel, block=block, steps=steps),
        grid_spec=pltpu.PrefetchScalarGridSpec(
            num_scalar_prefetch=1,
            grid=(steps,),
            in_specs=[
                whole(tok.shape), whole(ng.shape), whole(qw.shape), whole(kw.shape),
                whole(vw.shape), whole(fw.shape), whole(fb.shape), whole(qg.shape), whole(kg.shape),
                pl.BlockSpec((block, 1, hd, span), lambda i, *_: (i, 0, 0, 0)),
                pl.BlockSpec((block, 1, hd, span), lambda i, *_: (i, 0, 0, 0)),
                pl.BlockSpec((block, heads, span), lambda i, *_: (i, 0, 0)),
                whole(ow.shape),
            ],
            out_specs=[
                pl.BlockSpec(memory_space=pltpu.VMEM), whole((count, hd)), whole((count, hd)),
                whole((count, heads)),
            ],
            scratch_shapes=[
                pltpu.VMEM((rows, hd), BF16), pltpu.VMEM((rows, LANES), F32),
                pltpu.VMEM((rows, LANES), F32), pltpu.VMEM((rows, hd), F32),
                pltpu.VMEM((rows, hd), F32),
            ],
        ),
        out_shape=[
            jax.ShapeDtypeStruct((count, width), BF16), jax.ShapeDtypeStruct((count, hd), BF16),
            jax.ShapeDtypeStruct((count, hd), BF16), jax.ShapeDtypeStruct((count, heads), F32),
        ],
        compiler_params=params(60),
        name="attend",
    )(lens, tok, ng, qw, kw, vw, fw, fb, qg, kg, key, val, gate, ow)


def column(row, size):
    wide = jnp.broadcast_to(row, (size, size))
    return jnp.sum(jnp.where(iota((size, size), 0) == iota((size, size), 1), wide, 0), axis=1, keepdims=True)


def route_kernel(choice, info_out):
    count = choice.shape[1]
    picks = choice[...].astype(F32)
    earlier = iota((count, count), 1) < iota((count, count), 0)
    lane = iota((count, INFO), 1)
    info = jnp.zeros((count, INFO), F32)
    for k in range(SLOTS):
        mine_k = column(picks[k : k + 1, :], count)
        before = jnp.zeros((count, 1), F32)
        for other in range(SLOTS):
            same = jnp.logical_and(mine_k == picks[other : other + 1, :], earlier)
            before += jnp.sum(jnp.where(same, 1.0, 0.0), axis=1, keepdims=True)
        info = jnp.where(lane == k, mine_k * SLOTS + before, info)
    info_out[...] = info


def route(choice):
    out = jax.ShapeDtypeStruct((choice.shape[1], INFO), F32)
    return near_call(route_kernel, (choice,), out, limit=4)


def norm_kernel(tok, mine, theirs, pg, bg, info, copies, resid_out, branch_out):
    count, width = tok.shape
    half = width // 2
    second = lax.axis_index("tp") == 1
    attn = mine[...].astype(F32) + theirs[...].astype(F32)
    resid = (tok[...].astype(F32) + attn).astype(BF16).astype(F32)
    ms = jnp.mean(resid * resid, axis=1, keepdims=True)
    post = (resid * lax.rsqrt(ms + EPS) * laid_out(pg)).astype(BF16).astype(F32)
    line = jnp.concatenate(
        [jnp.where(second, post[:, half:], post[:, :half]), info[...]], axis=1
    ).astype(BF16)
    for peer in range(copies.shape[0]):
        copies[peer] = line
    logit = jnp.sum(post * laid_out(bg), axis=1, keepdims=True)
    branch_out[...] = jnp.broadcast_to(1.0 / (1.0 + jnp.exp(-logit)), (count, LANES))
    resid_out[...] = jnp.where(second, resid[:, half:], resid[:, :half])


def normalize(tok, mine, theirs, pg, bg, info, peers):
    count, width = tok.shape
    half = width // 2
    outs = [
        jax.ShapeDtypeStruct((peers, count, half + INFO), BF16),
        jax.ShapeDtypeStruct((count, half), F32),
        jax.ShapeDtypeStruct((count, LANES), F32),
    ]
    return near_call(norm_kernel, (tok, mine, theirs, pg, bg, info), outs, limit=8)


def hidden_kernel(x, *refs):
    (weights, (out, buf, sems)) = refs[:-3], refs[-3:]
    half, units = buf.shape[1:]
    rank = lax.axis_index("tp")
    moves = [
        pltpu.make_async_copy(
            w.at[pl.ds(pl.multiple_of(rank * half, half), half), :], buf.at[n], sems.at[n]
        )
        for n, w in enumerate(weights)
    ]
    for move in moves:
        move.start()
    tokens = x[:, :half]
    for b in range(len(weights) // 2):
        moves[2 * b].wait()
        moves[2 * b + 1].wait()
        w = jnp.concatenate([buf[2 * b], buf[2 * b + 1]], axis=1)
        out[:, 2 * units * b : 2 * units * (b + 1)] = mm(tokens, w).astype(BF16)


def dense_hidden(lines, weights):
    width, units = weights[0].shape
    here = pl.BlockSpec(memory_space=pltpu.VMEM)
    return pl.pallas_call(
        hidden_kernel,
        in_specs=[here] + [pl.BlockSpec(memory_space=pltpu.HBM)] * len(weights),
        out_specs=here,
        out_shape=jax.ShapeDtypeStruct((lines.shape[0], len(weights) * units), BF16),
        scratch_shapes=[
            pltpu.VMEM((len(weights), width // 2, units), BF16),
            pltpu.SemaphoreType.DMA((len(weights),)),
        ],
        compiler_params=params(16),
        name="dense_hidden",
    )(lines, *weights)


def extract_kernel(x, own_rows, near_rows, *, count):
    total = x.shape[0]
    half = own_rows.shape[1]
    peers = total // count
    shape = (total, 4 * peers)
    col = iota((1, 4 * peers), 1)
    expert = lax.axis_index("ep") ^ (col // (2 * peers))
    want = (expert * SLOTS + (col // peers) % 2).astype(F32)
    low = (col % peers) * count
    token = iota(shape, 0)
    info = x[:, half:].astype(F32)
    hit = jnp.logical_or(info[:, 0:1] == want, info[:, 1:2] == want)
    hit = jnp.logical_and(hit, jnp.logical_and(token >= low, token < low + count))
    pick = jnp.where(hit, 1.0, 0.0).astype(BF16)
    rows = lax.dot_general(
        pick, x[:, :half], (((0,), (0,)), ((), ())), preferred_element_type=F32
    ).astype(BF16)
    own_rows[...] = rows[: 2 * peers, :]
    near_rows[...] = rows[2 * peers :, :]


def extract(lines, count):
    total, wide = lines.shape
    rows = jax.ShapeDtypeStruct((2 * total // count, wide - INFO), BF16)
    kernel = functools.partial(extract_kernel, count=count)
    return near_call(kernel, (lines,), [rows, rows], limit=16)


def down_kernel(mine, theirs, *refs, count, block):
    weights, (far, squares, out, sems) = refs[:4], refs[4:]
    units = weights[0].shape[0]
    total, half = out.shape
    moves = []
    peers = total // count
    w = jnp.concatenate([kept(a, 1, half) for a in weights], axis=0)
    part = jnp.zeros((peers, LANES), F32)
    for step in range(total // block):
        at = slice(step * block, (step + 1) * block)

        def full(b):
            there = b ^ 1
            return mine[at, b * units : (b + 1) * units].astype(F32) + theirs[
                at, there * units : (there + 1) * units
            ].astype(F32)

        hidden = [silu(full(b)) * full(b + 2) for b in (0, 1, 4, 5)]
        square = jnp.sum(sum(h * h for h in hidden), axis=1, keepdims=True)
        h = jnp.concatenate([a.astype(BF16) for a in hidden], axis=1)
        out[at, :] = mm(h, w).astype(BF16)
        moves.append(pltpu.make_async_copy(out.at[at, :], far.at[at, :], sems.at[step]))
        moves[-1].start()
        token = iota((block, LANES), 0) + step * block
        spread = jnp.where(iota((block, LANES), 1) == token % count, square, 0.0)
        high = spread.astype(BF16)
        low = (spread - high.astype(F32)).astype(BF16)
        here = iota((peers, block), 1) + step * block
        start = iota((peers, block), 0) * count
        owner = jnp.logical_and(here >= start, here < start + count)
        owner = jnp.where(owner, 1.0, 0.0).astype(BF16)
        part += mm(owner, high) + mm(owner, low)
    squares[...] = part
    for move in moves:
        move.wait()


def dense_down(mine, theirs, weights, count):
    total = mine.shape[0]
    half = weights[0].shape[1] // 2
    block = 256
    here = pl.BlockSpec(memory_space=pltpu.VMEM)
    return pl.pallas_call(
        functools.partial(down_kernel, count=count, block=block),
        in_specs=[here] * (2 + len(weights)),
        out_specs=[pl.BlockSpec(memory_space=pltpu.HBM), here],
        out_shape=[
            jax.ShapeDtypeStruct((total, half), BF16),
            jax.ShapeDtypeStruct((total // count, LANES), F32),
        ],
        scratch_shapes=[
            pltpu.VMEM((total, half), BF16), pltpu.SemaphoreType.DMA((total // block,)),
        ],
        compiler_params=params(16),
        name="dense_down",
    )(mine, theirs, *weights)


def expert_kernel(a0, b0, a1, b1, gw, uw, dw, after, keep, give, gbuf, ubuf, dbuf, sems):
    half = a0.shape[1]
    moves = []
    for n, (far, buf) in enumerate(((gw, gbuf), (uw, ubuf), (dw, dbuf))):
        part = buf.shape[0] // 2
        for m in range(2):
            at = pl.ds(m * part, part)
            moves.append(pltpu.make_async_copy(far.at[0, at, :], buf.at[at, :], sems.at[2 * n + m]))
            moves[-1].start()
    x0 = jnp.concatenate([a0[...], b0[...]], axis=0)
    x1 = jnp.concatenate([a1[...], b1[...]], axis=0)

    def rows(w):
        return mm(x0, kept(w, 0, half)) + mm(x1, kept(w, 0, half, True))

    moves[0].wait()
    moves[1].wait()
    gate = silu(rows(gbuf))
    moves[2].wait()
    moves[3].wait()
    act = (gate * rows(ubuf)).astype(BF16)
    moves[4].wait()
    moves[5].wait()
    keep[...] = mm(act, kept(dbuf, 1, half)).astype(BF16)
    give[...] = mm(act, kept(dbuf, 1, half, True)).astype(BF16)


def experts(rows, away, gate_w, up_w, down_w, after):
    count, half = rows[0].shape
    here = pl.BlockSpec(memory_space=pltpu.VMEM)
    far = pl.BlockSpec(memory_space=pltpu.HBM)
    return pl.pallas_call(
        expert_kernel,
        in_specs=[here] * 4 + [far] * 3 + [here],
        out_specs=[here] * 2,
        out_shape=[jax.ShapeDtypeStruct((2 * count, half), BF16)] * 2,
        scratch_shapes=[pltpu.VMEM(w.shape[1:], BF16) for w in (gate_w, up_w, down_w)]
        + [pltpu.SemaphoreType.DMA((6,))],
        compiler_params=params(24),
        name="experts",
    )(*rows, *away, gate_w, up_w, down_w, after)


def answer_kernel(keep, other, squares, out, scr):
    mine = class_of(lax.axis_index("ep"))
    peers = out.shape[0]
    total = keep[...].astype(F32) + other[...].astype(F32)
    parts = total.shape[1] // LANES
    for q in range(2):
        for s in range(SLOTS):
            own = total[peers * s : peers * (s + 1), :]
            near = total[2 * peers + peers * s : 2 * peers + peers * (s + 1), :]
            rows = jnp.where((iota((peers, 1), 0) + q) % 2 == mine, own, near)
            for f in range(parts):
                scr[:, parts * s + f, :] = rows[:, LANES * f : LANES * (f + 1)]
        out[:, q, : SLOTS * parts, :] = scr[...].astype(BF16)
        line = jnp.where((iota((peers, 1), 0) + q) % 2 == mine, squares[...], 0.0)
        out[:, q, SLOTS * parts :, :] = jnp.broadcast_to(line[:, None, :], (peers, 8, LANES)).astype(BF16)


def answers(keep, other, squares):
    peers = squares.shape[0]
    half = keep.shape[1]
    rows = SLOTS * half // LANES
    out = jax.ShapeDtypeStruct((peers, 2, rows + 8, LANES), BF16)
    scratch = [pltpu.VMEM((peers, rows, LANES), F32)]
    return near_call(answer_kernel, (keep, other, squares), out, scratch, limit=16)


def last_kernel(returned, parts, info, weight, branch, resid, out, scr):
    count, half = resid.shape
    ep = returned.shape[0]
    tiles = half // LANES
    rows = SLOTS * tiles
    scr[...] = returned[:, :rows, :].astype(F32)
    values = jnp.concatenate(
        [
            jnp.concatenate([scr[:, tiles * s + f, :] for f in range(tiles)], axis=1)
            for s in range(SLOTS)
        ],
        axis=0,
    ).astype(BF16)
    lane = iota((count, SLOTS * ep), 1)
    code = ((lane % ep) * SLOTS + lane // ep).astype(F32)
    expert_sum = jnp.zeros((count, half), F32)
    for k in range(SLOTS):
        pick = jnp.where(info[:, k : k + 1] == code, 1.0, 0.0).astype(BF16)
        expert_sum += column(weight[k : k + 1, :], count) * mm(pick, values)
    square = jnp.sum(returned[:, rows : rows + 8, :].astype(F32), axis=0)
    square = column(square[0:1, :count], count)
    dense = jnp.sum(parts[...].astype(F32), axis=0)
    dense = (dense * lax.rsqrt(square / FF2 + EPS)).astype(BF16).astype(F32)
    out[...] = (resid[...] + expert_sum + branch[:, :1] * dense).astype(BF16)


def last_sum(returned, parts, info, weight, branch, resid):
    arrays = (returned, parts, info, weight, branch, resid)
    out = jax.ShapeDtypeStruct(resid.shape, BF16)
    scratch = [pltpu.VMEM((returned.shape[0], SLOTS * resid.shape[1] // LANES, LANES), F32)]
    return near_call(last_kernel, arrays, out, scratch, limit=16)


def body(
    tokens,
    norm_gain,
    query_w,
    key_w,
    value_w,
    forget_w,
    forget_bias,
    query_gain,
    key_gain,
    cache_key,
    cache_value,
    cache_gate,
    cache_len,
    out_w,
    post_gain,
    branch_gate,
    dense_gate_w,
    dense_up_w,
    dense_down_w,
    expert_choice,
    route_weight,
    expert_gate_w,
    expert_up_w,
    expert_down_w,
):
    count = tokens.shape[0]
    ep_count = lax.axis_size("ep")
    peers = ep_count // 2
    pair = [(e, e ^ 1) for e in range(ep_count)]
    classes = [[e for e in range(ep_count) if class_of(e) == c] for c in range(2)]

    near = []
    for array in (dense_gate_w, dense_up_w, dense_down_w):
        near.append(lax.ppermute(array, "ep", pair))

    partial, fresh_key, fresh_value, current = attend(
        cache_len, tokens, tiled(norm_gain), query_w, key_w, value_w, forget_w.T,
        forget_bias[None], query_gain[None], key_gain[None], cache_key, cache_value,
        cache_gate, out_w,
    )
    partial_other = swapped(partial)
    info = route(expert_choice.T)
    copies, resid, branch = normalize(
        tokens, partial, partial_other, tiled(post_gain), tiled(branch_gate), info, peers
    )
    lines = lax.all_to_all(copies, "ep", 0, 0, tiled=True, axis_index_groups=classes)
    lines = lines.reshape(peers * count, -1)

    gate_up = []
    for gate_w, up_w in ((dense_gate_w, dense_up_w), (near[0], near[1])):
        gate_up += [gate_w, swapped(gate_w), up_w, swapped(up_w)]
    downs = []
    for down_w in (dense_down_w, near[2]):
        downs += [down_w, swapped(down_w)]

    part = dense_hidden(lines, gate_up)
    part_other = swapped(part)
    own_rows, near_rows = extract(lines, count)
    pair_rows = lax.ppermute(near_rows, "ep", pair)
    terms, squares = dense_down(part, part_other, downs, count)
    parts = lax.all_to_all(
        terms.reshape(peers, count, -1), "ep", 0, 0, tiled=True, axis_index_groups=classes
    )

    away = (swapped(own_rows), swapped(pair_rows))
    keep, give = experts(
        (own_rows, pair_rows), away, expert_gate_w, expert_up_w, expert_down_w, squares
    )
    answer = answers(keep, swapped(give), squares)
    returned = lax.all_to_all(answer.reshape(ep_count, *answer.shape[2:]), "ep", 0, 0, tiled=True)
    mixed_out = last_sum(returned, parts, info, route_weight.T, branch, resid)
    return (mixed_out, fresh_key[:, None, :], fresh_value[:, None, :], current)


def solution(mesh):
    placed = (
        P("ep", None),
        P(),
        P(None, "tp"),
        P(),
        P(),
        P(),
        P(),
        P(),
        P(),
        P("ep", "tp", None, None),
        P("ep", "tp", None, None),
        P("ep", "tp", None),
        P("ep"),
        P("tp", None),
        P(),
        P(),
        P(None, ("ep", "tp")),
        P(None, ("ep", "tp")),
        P(("ep", "tp"), None),
        P("ep", None),
        P("ep", None),
        P("ep", None, "tp"),
        P("ep", None, "tp"),
        P("ep", "tp", None),
    )

    return jax.shard_map(
        body,
        mesh=mesh,
        in_specs=placed,
        out_specs=(P("ep", "tp"), P("ep", "tp", None), P("ep", "tp", None), P("ep", "tp")),
        check_vma=False,
    )
```

profile of v0, /device:TPU:0, one launch (start us, length us, event | category | flops | bytes accessed | tf_op | source)
XLA Modules:
  0.0 143.8 jit_solution(10238197736442956452)
XLA Ops:
  0.6 0.0 copy-start.21
  0.7 10.8 %attend.1 = (bf16[24,2048]{1,0:T(8,128)(2,1)}, bf16[24,64]{1,0:T(8,128)(2,1)}, bf16[24,64]{1,0:T(8,128)(2,1)}, f32[24,8]{1,0:T(8,128)}) custom-call(s32[24]{0:T(128)} %len_ref.1, bf16[24,2048]{1,0:T(8,128)(2,1)} %tok.3, bf16[16,128]{1,0:T(8,128)(2,1)} %bitcast.22, bf16[2048,512]{1,0:T(8,128)(2,1)} %qw.1, bf16[2048,128]{1,0:T(8,128)(2,1)} %kw.1, ...), custom_call_target="tpu_custom_call" | custom-call | tf_op jit(solution)/shard_map/attend/pallas_call | solution.py:178
  11.4 0.0 copy-start.3
  11.5 0.0 copy-start.4
  11.5 0.1 collective-permute-start
  11.6 0.2 shard_map.255.info
  11.7 1.3 collective-permute-done.theirs
  13.1 0.0 copy-done.18
  13.1 0.9 copy-done.17
  14.0 1.5 %shard_map.256 = (bf16[32,24,1152]{2,1,0:T(8,128)(2,1)}, f32[24,1024]{1,0:T(8,128)S(1)}, f32[24,128]{1,0:T(8,128)S(1)}) custom-call(bf16[24,2048]{1,0:T(8,128)(2,1)S(1)} %copy-done.16, bf16[24,2048]{1,0:T(8,128)(2,1)S(1)} %copy-done.17, bf16[24,2048]{1,0:T(8,128)(2,1)S(1)} %collective-permute-done.theirs, bf16[16,128]{1,0:T(8,128)(2,1)S(1)} %bitcast.17, ...), custom_call_target="tpu_custom_call" | custom-call | tf_op jit(solution)/shard_map/pallas_call | solution.py:56
  15.5 10.6 %all-to-all-start = ((bf16[32,24,1152]{2,1,0:T(8,128)(2,1)}), bf16[32,24,1152]{2,1,0:T(8,128)(2,1)S(1)}, u32[]{:S(2)}, u32[]{:S(2)}) async-start(bf16[32,24,1152]{2,1,0:T(8,128)(2,1)} %get-tuple-element.18), calls=%async_computation | async-start | bytes 3538944 | tf_op jit(solution)/shard_map/all_to_all | solution.py:536
  26.1 0.0 copy-done.3
  26.1 0.3 collective-permute-start.6
  26.4 1.8 %collective-permute-start.8 = (bf16[2048,128]{1,0:T(8,128)(2,1)S(1)}, bf16[2048,128]{1,0:T(8,128)(2,1)S(1)}, u32[]{:S(2)}, u32[]{:S(2)}) collective-permute-start(bf16[2048,128]{1,0:T(8,128)(2,1)S(1)} %copy-done.4), channel_id=1, source_target_pairs={{0,2},{2,0},{4,6},{6,4},{8,10},{10,8},{12,14},{14,12},{16,18},{18,... | collective-permute-start | bytes 1572872 | tf_op jit(solution)/shard_map/ppermute | solution.py:524
  28.2 0.0 collective-permute-start.4
  28.2 0.5 collective-permute-start.5
  28.8 12.3 %collective-permute-done.6.refs_4_ = bf16[2048,128]{1,0:T(8,128)(2,1)S(1)} collective-permute-done((bf16[2048,128]{1,0:T(8,128)(2,1)S(1)}, bf16[2048,128]{1,0:T(8,128)(2,1)S(1)}, u32[]{:S(2)}, u32[]{:S(2)}) %collective-permute-start.6) | collective-permute-done | bytes 524320 | tf_op jit(solution)/shard_map/ppermute | solution.py:524
  41.0 0.0 collective-permute-start.7
  41.0 10.1 %collective-permute-done.8.refs_6_ = bf16[2048,128]{1,0:T(8,128)(2,1)S(1)} collective-permute-done((bf16[2048,128]{1,0:T(8,128)(2,1)S(1)}, bf16[2048,128]{1,0:T(8,128)(2,1)S(1)}, u32[]{:S(2)}, u32[]{:S(2)}) %collective-permute-start.8) | collective-permute-done | bytes 524320 | tf_op jit(solution)/shard_map/ppermute | solution.py:524
  51.1 0.0 collective-permute-start.9
  51.2 0.8 copy-done.5
  51.9 0.0 collective-permute-done.4.refs_1_
  51.9 0.8 copy-done.7
  52.7 0.0 collective-permute-done.5.refs_3_
  52.7 0.8 copy-done.9
  53.5 0.0 collective-permute-done.7.refs_5_
  53.5 0.8 copy-done.11
  54.3 0.0 collective-permute-done.9.refs_7_
  54.4 0.8 copy-done.13
  55.2 0.0 all-to-all-done
  55.2 1.0 copy-done.6
  56.2 1.0 copy-done.8
  57.2 1.0 copy-done.10
  58.3 1.0 copy-done.12
  59.3 1.0 copy-done.14
  60.4 4.2 %dense_hidden.1.mine = bf16[768,1024]{1,0:T(8,128)(2,1)S(1)} custom-call(bf16[768,1152]{1,0:T(8,128)(2,1)S(1)} %bitcast.14, bf16[2048,128]{1,0:T(8,128)(2,1)S(1)} %copy-done.3, bf16[2048,128]{1,0:T(8,128)(2,1)S(1)} %copy-done.8, bf16[2048,128]{1,0:T(8,128)(2,1)S(1)} %copy-done.4, bf16[2048,128]{1,0:T(8,128)(2,1)S(1)} %copy-done.10, ...), custom_call_target="tpu_custom_call" | custom-call | tf_op jit(solution)/shard_map/dense_hidden/pallas_call | solution.py:288
  64.5 0.6 collective-permute-start.10
  65.1 0.3 collective-permute-start.12
  65.4 0.0 collective-permute-start.11
  65.4 13.6 %collective-permute-done.12.refs_2_ = bf16[128,2048]{1,0:T(8,128)(2,1)S(1)} collective-permute-done((bf16[128,2048]{1,0:T(8,128)(2,1)S(1)}, bf16[128,2048]{1,0:T(8,128)(2,1)S(1)}, u32[]{:S(2)}, u32[]{:S(2)}) %collective-permute-start.12) | collective-permute-done | bytes 524320 | tf_op jit(solution)/shard_map/ppermute | solution.py:524
  79.1 0.0 collective-permute-start.13
  79.1 0.6 shard_map.257
  79.7 0.4 collective-permute-start.1
  80.1 0.3 collective-permute-start.2
  80.4 5.3 %collective-permute-done.1.b0 = bf16[64,1024]{1,0:T(8,128)(2,1)S(1)} collective-permute-done((bf16[64,1024]{1,0:T(8,128)(2,1)S(1)}, bf16[64,1024]{1,0:T(8,128)(2,1)S(1)}, u32[]{:S(2)}, u32[]{:S(2)}) %collective-permute-start.1) | collective-permute-done | bytes 131104 | tf_op jit(solution)/shard_map/ppermute | solution.py:549
  85.7 0.0 collective-permute-start.3
  85.7 0.0 collective-permute-done.11.refs_1_
  85.7 0.0 collective-permute-done.13.refs_3_
  85.7 0.0 collective-permute-done.10.theirs
  85.7 2.3 %dense_down.1 = (bf16[768,1024]{1,0:T(8,128)(2,1)}, f32[32,128]{1,0:T(8,128)S(1)}) custom-call(bf16[768,1024]{1,0:T(8,128)(2,1)S(1)} %dense_hidden.1.mine, bf16[768,1024]{1,0:T(8,128)(2,1)S(1)} %collective-permute-done.10.theirs, bf16[128,2048]{1,0:T(8,128)(2,1)S(1)} %copy-done.15, bf16[128,2048]{1,0:T(8,128)(2,1)S(1)} %collective-permute-done.11.refs_1_, ...), custom_call_target="tpu_custom_call" | custom-call | tf_op jit(solution)/shard_map/dense_down/pallas_call | solution.py:372
  88.0 0.0 collective-permute-done.2.a1
  88.0 0.0 collective-permute-done.3.b1
  88.0 1.9 %experts.1 = (bf16[128,1024]{1,0:T(8,128)(2,1)S(1)}, bf16[128,1024]{1,0:T(8,128)(2,1)S(1)}) custom-call(bf16[64,1024]{1,0:T(8,128)(2,1)S(1)} %get-tuple-element.19.a0, bf16[64,1024]{1,0:T(8,128)(2,1)S(1)} %collective-permute-done.1.b0, bf16[64,1024]{1,0:T(8,128)(2,1)S(1)} %collective-permute-done.2.a1, bf16[64,1024]{1,0:T(8,128)(2,1)S(1)} %collective-permute-done.3.b1, ...), custom_call_target="tpu_custom_call" | custom-call | tf_op jit(solution)/shard_map/experts/pallas_call | solution.py:419
  89.9 0.8 collective-permute-start.14
  90.7 1.2 collective-permute-done.14.other
  91.9 0.5 shard_map.258
  92.4 0.0 copy-start.22
  92.4 0.0 copy-start.20
  92.4 22.2 %all_to_all.15.returned = bf16[64,24,128]{2,1,0:T(8,128)(2,1)S(1)} all-to-all(bf16[64,24,128]{2,1,0:T(8,128)(2,1)S(1)} %bitcast.16), channel_id=1, replica_groups=mesh['ep'=64,'tp'=2] {'ep'}, dimensions={0} | all-to-all | bytes 786432 | tf_op jit(solution)/shard_map/all_to_all | solution.py:560
  114.5 4.0 %all-to-all-start.2 = ((bf16[32,24,1024]{2,1,0:T(8,128)(2,1)}), bf16[32,24,1024]{2,1,0:T(8,128)(2,1)S(1)}, u32[]{:S(2)}, u32[]{:S(2)}) async-start(bf16[32,24,1024]{2,1,0:T(8,128)(2,1)} %bitcast.10), calls=%async_computation.2 | async-start | bytes 3145728 | tf_op jit(solution)/shard_map/all_to_all | solution.py:551
  118.5 0.0 copy-done.22
  118.5 0.7 copy.28
  119.2 23.4 %all-to-all-done.2.parts = bf16[32,24,1024]{2,1,0:T(8,128)(2,1)S(1)} async-done(((bf16[32,24,1024]{2,1,0:T(8,128)(2,1)}), bf16[32,24,1024]{2,1,0:T(8,128)(2,1)S(1)}, u32[]{:S(2)}, u32[]{:S(2)}) %all-to-all-start.2) | async-done | bytes 1572896 | tf_op jit(solution)/shard_map/all_to_all | solution.py:551
  142.6 1.3 shard_map.259
  (27 shorter events, 0.0 us)
Async XLA Ops:
  0.6 10.9 %copy-start.21 = (s32[24,2]{0,1:T(2,128)S(1)}, s32[24,2]{0,1:T(2,128)}, u32[]{:S(2)}) copy-start(s32[24,2]{0,1:T(2,128)} %param.43) | copy-start | bytes 580
  0.6 12.4 %copy-start.16 = (bf16[24,2048]{1,0:T(8,128)(2,1)S(1)}, bf16[24,2048]{1,0:T(8,128)(2,1)}, u32[]{:S(2)}) copy-start(bf16[24,2048]{1,0:T(8,128)(2,1)} %tok.3) | copy-start | bytes 294916
  0.7 12.4 %copy-start.18 = (bf16[2048]{0:T(1024)(128)(2,1)S(1)}, bf16[2048]{0:T(1024)(128)(2,1)}, u32[]{:S(2)}) copy-start(bf16[2048]{0:T(1024)(128)(2,1)} %param.38) | copy-start | bytes 12292
  0.7 12.4 %copy-start.19 = (bf16[2048]{0:T(1024)(128)(2,1)S(1)}, bf16[2048]{0:T(1024)(128)(2,1)}, u32[]{:S(2)}) copy-start(bf16[2048]{0:T(1024)(128)(2,1)} %param.39) | copy-start | bytes 12292
  11.4 14.7 %copy-start.3 = (bf16[2048,128]{1,0:T(8,128)(2,1)S(1)}, bf16[2048,128]{1,0:T(8,128)(2,1)}, u32[]{:S(2)}) copy-start(bf16[2048,128]{1,0:T(8,128)(2,1)} %refs_0_.2) | copy-start | bytes 1572868
  11.5 15.0 %copy-start.4 = (bf16[2048,128]{1,0:T(8,128)(2,1)S(1)}, bf16[2048,128]{1,0:T(8,128)(2,1)}, u32[]{:S(2)}) copy-start(bf16[2048,128]{1,0:T(8,128)(2,1)} %refs_2_.1) | copy-start | bytes 1572868
  11.5 1.6 %collective-permute-start = (bf16[24,2048]{1,0:T(8,128)(2,1)}, bf16[24,2048]{1,0:T(8,128)(2,1)S(1)}, u32[]{:S(2)}, u32[]{:S(2)}) collective-permute-start(bf16[24,2048]{1,0:T(8,128)(2,1)} %get-tuple-element.17.mine), channel_id=1, source_target_pairs={{0,1},{1,0},{2,3},{3,2},{4,5},{5,4},{6,7},{7,6},{8,9},{9,8},{10,11... | collective-permute-start | bytes 294920 | tf_op jit(solution)/shard_map/ppermute | solution.py:26
  13.1 0.9 copy-start.17
  15.5 39.7 %all-to-all-start = ((bf16[32,24,1152]{2,1,0:T(8,128)(2,1)}), bf16[32,24,1152]{2,1,0:T(8,128)(2,1)S(1)}, u32[]{:S(2)}, u32[]{:S(2)}) async-start(bf16[32,24,1152]{2,1,0:T(8,128)(2,1)} %get-tuple-element.18), calls=%async_computation | async-start | bytes 3538944 | tf_op jit(solution)/shard_map/all_to_all | solution.py:536
  26.1 14.9 %collective-permute-start.6 = (bf16[2048,128]{1,0:T(8,128)(2,1)S(1)}, bf16[2048,128]{1,0:T(8,128)(2,1)S(1)}, u32[]{:S(2)}, u32[]{:S(2)}) collective-permute-start(bf16[2048,128]{1,0:T(8,128)(2,1)S(1)} %copy-done.3), channel_id=1, source_target_pairs={{0,2},{2,0},{4,6},{6,4},{8,10},{10,8},{12,14},{14,12},{16,18},{18,... | collective-permute-start | bytes 1572872 | tf_op jit(solution)/shard_map/ppermute | solution.py:524
  26.4 24.7 %collective-permute-start.8 = (bf16[2048,128]{1,0:T(8,128)(2,1)S(1)}, bf16[2048,128]{1,0:T(8,128)(2,1)S(1)}, u32[]{:S(2)}, u32[]{:S(2)}) collective-permute-start(bf16[2048,128]{1,0:T(8,128)(2,1)S(1)} %copy-done.4), channel_id=1, source_target_pairs={{0,2},{2,0},{4,6},{6,4},{8,10},{10,8},{12,14},{14,12},{16,18},{18,... | collective-permute-start | bytes 1572872 | tf_op jit(solution)/shard_map/ppermute | solution.py:524
  28.2 23.7 %collective-permute-start.4 = (bf16[2048,128]{1,0:T(8,128)(2,1)S(1)}, bf16[2048,128]{1,0:T(8,128)(2,1)S(1)}, u32[]{:S(2)}, u32[]{:S(2)}) collective-permute-start(bf16[2048,128]{1,0:T(8,128)(2,1)S(1)} %copy-done.3), channel_id=1, source_target_pairs={{0,1},{1,0},{2,3},{3,2},{4,5},{5,4},{6,7},{7,6},{8,9},{9,8},{10,11... | collective-permute-start | bytes 1572872 | tf_op jit(solution)/shard_map/ppermute | solution.py:26
  28.2 24.5 %collective-permute-start.5 = (bf16[2048,128]{1,0:T(8,128)(2,1)S(1)}, bf16[2048,128]{1,0:T(8,128)(2,1)S(1)}, u32[]{:S(2)}, u32[]{:S(2)}) collective-permute-start(bf16[2048,128]{1,0:T(8,128)(2,1)S(1)} %copy-done.4), channel_id=1, source_target_pairs={{0,1},{1,0},{2,3},{3,2},{4,5},{5,4},{6,7},{7,6},{8,9},{9,8},{10,11... | collective-permute-start | bytes 1572872 | tf_op jit(solution)/shard_map/ppermute | solution.py:26
  41.0 12.5 %collective-permute-start.7 = (bf16[2048,128]{1,0:T(8,128)(2,1)S(1)}, bf16[2048,128]{1,0:T(8,128)(2,1)S(1)}, u32[]{:S(2)}, u32[]{:S(2)}) collective-permute-start(bf16[2048,128]{1,0:T(8,128)(2,1)S(1)} %collective-permute-done.6.refs_4_), channel_id=1, source_target_pairs={{0,1},{1,0},{2,3},{3,2},{4,5},{5,4},{6,7},{7,6},{8,9},{9,8},{10,11... | collective-permute-start | bytes 1572872 | tf_op jit(solution)/shard_map/ppermute | solution.py:26
  51.1 3.2 %collective-permute-start.9 = (bf16[2048,128]{1,0:T(8,128)(2,1)S(1)}, bf16[2048,128]{1,0:T(8,128)(2,1)S(1)}, u32[]{:S(2)}, u32[]{:S(2)}) collective-permute-start(bf16[2048,128]{1,0:T(8,128)(2,1)S(1)} %collective-permute-done.8.refs_6_), channel_id=1, source_target_pairs={{0,1},{1,0},{2,3},{3,2},{4,5},{5,4},{6,7},{7,6},{8,9},{9,8},{10,11... | collective-permute-start | bytes 1572872 | tf_op jit(solution)/shard_map/ppermute | solution.py:26
  51.2 0.8 copy-start.5
  51.9 0.8 copy-start.7
  52.7 0.8 copy-start.9
  53.5 0.8 copy-start.11
  54.3 0.8 copy-start.13
  55.2 1.0 copy-start.6
  56.2 1.0 copy-start.8
  57.2 1.0 copy-start.10
  58.3 1.0 copy-start.12
  59.3 1.0 copy-start.14
  60.4 4.8 %copy-start.15 = (bf16[128,2048]{1,0:T(8,128)(2,1)S(1)}, bf16[128,2048]{1,0:T(8,128)(2,1)}, u32[]{:S(2)}) copy-start(bf16[128,2048]{1,0:T(8,128)(2,1)} %refs_0_.3) | copy-start | bytes 1572868
  64.5 21.1 %collective-permute-start.10 = (bf16[768,1024]{1,0:T(8,128)(2,1)S(1)}, bf16[768,1024]{1,0:T(8,128)(2,1)S(1)}, u32[]{:S(2)}, u32[]{:S(2)}) collective-permute-start(bf16[768,1024]{1,0:T(8,128)(2,1)S(1)} %dense_hidden.1.mine), channel_id=1, source_target_pairs={{0,1},{1,0},{2,3},{3,2},{4,5},{5,4},{6,7},{7,6},{8,9},{9,8},{10,11... | collective-permute-start | bytes 4718600 | tf_op jit(solution)/shard_map/ppermute | solution.py:26
  65.1 13.9 %collective-permute-start.12 = (bf16[128,2048]{1,0:T(8,128)(2,1)S(1)}, bf16[128,2048]{1,0:T(8,128)(2,1)S(1)}, u32[]{:S(2)}, u32[]{:S(2)}) collective-permute-start(bf16[128,2048]{1,0:T(8,128)(2,1)S(1)} %copy-done.15), channel_id=1, source_target_pairs={{0,2},{2,0},{4,6},{6,4},{8,10},{10,8},{12,14},{14,12},{16,18},{18,... | collective-permute-start | bytes 1572872 | tf_op jit(solution)/shard_map/ppermute | solution.py:524
  65.4 20.3 %collective-permute-start.11 = (bf16[128,2048]{1,0:T(8,128)(2,1)S(1)}, bf16[128,2048]{1,0:T(8,128)(2,1)S(1)}, u32[]{:S(2)}, u32[]{:S(2)}) collective-permute-start(bf16[128,2048]{1,0:T(8,128)(2,1)S(1)} %copy-done.15), channel_id=1, source_target_pairs={{0,1},{1,0},{2,3},{3,2},{4,5},{5,4},{6,7},{7,6},{8,9},{9,8},{10,11... | collective-permute-start | bytes 1572872 | tf_op jit(solution)/shard_map/ppermute | solution.py:26
  79.1 6.6 %collective-permute-start.13 = (bf16[128,2048]{1,0:T(8,128)(2,1)S(1)}, bf16[128,2048]{1,0:T(8,128)(2,1)S(1)}, u32[]{:S(2)}, u32[]{:S(2)}) collective-permute-start(bf16[128,2048]{1,0:T(8,128)(2,1)S(1)} %collective-permute-done.12.refs_2_), channel_id=1, source_target_pairs={{0,1},{1,0},{2,3},{3,2},{4,5},{5,4},{6,7},{7,6},{8,9},{9,8},{10,11... | collective-permute-start | bytes 1572872 | tf_op jit(solution)/shard_map/ppermute | solution.py:26
  79.1 8.9 %copy-start.2 = (bf16[1,512,2048]{2,1,0:T(8,128)(2,1)S(1)}, bf16[1,512,2048]{2,1,0:T(8,128)(2,1)}, u32[]{:S(2)}) copy-start(bf16[1,512,2048]{2,1,0:T(8,128)(2,1)} %dw.1) | copy-start | bytes 6291460
  79.7 6.0 %collective-permute-start.1 = (bf16[64,1024]{1,0:T(8,128)(2,1)S(1)}, bf16[64,1024]{1,0:T(8,128)(2,1)S(1)}, u32[]{:S(2)}, u32[]{:S(2)}) collective-permute-start(bf16[64,1024]{1,0:T(8,128)(2,1)S(1)} %get-tuple-element.20), channel_id=1, source_target_pairs={{0,2},{2,0},{4,6},{6,4},{8,10},{10,8},{12,14},{14,12},{16,18},{18,... | collective-permute-start | bytes 393224 | tf_op jit(solution)/shard_map/ppermute | solution.py:549
  80.1 7.9 %copy-start = (bf16[1,2048,512]{2,1,0:T(8,128)(2,1)S(1)}, bf16[1,2048,512]{2,1,0:T(8,128)(2,1)}, u32[]{:S(2)}) copy-start(bf16[1,2048,512]{2,1,0:T(8,128)(2,1)} %gw.1) | copy-start | bytes 6291460
  80.1 7.9 %copy-start.1 = (bf16[1,2048,512]{2,1,0:T(8,128)(2,1)S(1)}, bf16[1,2048,512]{2,1,0:T(8,128)(2,1)}, u32[]{:S(2)}) copy-start(bf16[1,2048,512]{2,1,0:T(8,128)(2,1)} %uw.1) | copy-start | bytes 6291460
  80.1 7.9 %collective-permute-start.2 = (bf16[64,1024]{1,0:T(8,128)(2,1)S(1)}, bf16[64,1024]{1,0:T(8,128)(2,1)S(1)}, u32[]{:S(2)}, u32[]{:S(2)}) collective-permute-start(bf16[64,1024]{1,0:T(8,128)(2,1)S(1)} %get-tuple-element.19.a0), channel_id=1, source_target_pairs={{0,1},{1,0},{2,3},{3,2},{4,5},{5,4},{6,7},{7,6},{8,9},{9,8},{10,11... | collective-permute-start | bytes 393224 | tf_op jit(solution)/shard_map/ppermute | solution.py:26
  85.7 2.3 %collective-permute-start.3 = (bf16[64,1024]{1,0:T(8,128)(2,1)S(1)}, bf16[64,1024]{1,0:T(8,128)(2,1)S(1)}, u32[]{:S(2)}, u32[]{:S(2)}) collective-permute-start(bf16[64,1024]{1,0:T(8,128)(2,1)S(1)} %collective-permute-done.1.b0), channel_id=1, source_target_pairs={{0,1},{1,0},{2,3},{3,2},{4,5},{5,4},{6,7},{7,6},{8,9},{9,8},{10,11... | collective-permute-start | bytes 393224 | tf_op jit(solution)/shard_map/ppermute | solution.py:26
  89.9 1.9 %collective-permute-start.14 = (bf16[128,1024]{1,0:T(8,128)(2,1)S(1)}, bf16[128,1024]{1,0:T(8,128)(2,1)S(1)}, u32[]{:S(2)}, u32[]{:S(2)}) collective-permute-start(bf16[128,1024]{1,0:T(8,128)(2,1)S(1)} %get-tuple-element.23), channel_id=1, source_target_pairs={{0,1},{1,0},{2,3},{3,2},{4,5},{5,4},{6,7},{7,6},{8,9},{9,8},{10,11... | collective-permute-start | bytes 786440 | tf_op jit(solution)/shard_map/ppermute | solution.py:26
  92.4 26.2 %copy-start.22 = (f32[24,8]{1,0:T(8,128)S(1)}, f32[24,8]{1,0:T(8,128)}, u32[]{:S(2)}) copy-start(f32[24,8]{1,0:T(8,128)} %get-tuple-element.33) | copy-start | bytes 2308
  92.4 50.2 %copy-start.20 = (f32[24,2]{0,1:T(2,128)S(1)}, f32[24,2]{0,1:T(2,128)}, u32[]{:S(2)}) copy-start(f32[24,2]{0,1:T(2,128)} %param.44) | copy-start | bytes 580
  114.5 28.0 %all-to-all-start.2 = ((bf16[32,24,1024]{2,1,0:T(8,128)(2,1)}), bf16[32,24,1024]{2,1,0:T(8,128)(2,1)S(1)}, u32[]{:S(2)}, u32[]{:S(2)}) async-start(bf16[32,24,1024]{2,1,0:T(8,128)(2,1)} %bitcast.10), calls=%async_computation.2 | async-start | bytes 3145728 | tf_op jit(solution)/shard_map/all_to_all | solution.py:551
where the time goes:
time: 145 us; the launch traced here: 144 us
  waiting for transfers between devices  67.2 us (46%)
  Pallas kernels  23.2 us (16%)
  blocking collectives  22.2 us (15%)
  starting transfers between devices  19.7 us (14%)
  local copies, waits for them, and re-layouts  10.8 us (7%)
    ppermute x3, waiting for transfers between devices, body(): near.append(lax.ppermute(array, 'ep', pair))  36 us
    all_to_all x1, waiting for transfers between devices, body(): lax.all_to_all(terms.reshape(peers, count, -1), 'ep', 0, 0, tiled=True, a...  23.4 us
    all_to_all x1, blocking collectives, body(): lax.all_to_all(answer.reshape(ep_count, *answer.shape[2:]), 'ep', 0, 0, t...  22.2 us
    unnamed x47, local copies, waits for them, and re-layouts  10.8 us
    pallas_call x1, Pallas kernels, attend(): pl.pallas_call(functools.partial(attend_kernel, block=block, steps=steps)...  10.8 us
    all_to_all x1, starting transfers between devices, body(): lax.all_to_all(copies, 'ep', 0, 0, tiled=True, axis_index_groups=classes)  10.6 us
    ppermute x1, waiting for transfers between devices, body(): pair_rows = lax.ppermute(near_rows, 'ep', pair)  5.28 us
    pallas_call x1, Pallas kernels, dense_hidden(): pl.pallas_call(hidden_kernel, in_specs=[here] + [pl.BlockSpec(memory_spac...  4.16 us
  transfers between devices with their start and end apart: 17, of which 7 were waited for; matrix products, arithmetic and copies ran while one was open for 0% of the time, Pallas kernels for 2%

commit v1 on v0

v1 whole, which is shorter than its diff:
```python
import functools

import jax
import jax.numpy as jnp
from jax import lax
from jax.experimental import pallas as pl
from jax.experimental.pallas import tpu as pltpu
from jax.sharding import PartitionSpec as P


FF2 = 16384
LANES = 128
INFO = 128
SLOTS = 2
EPS = 1e-06
SWAP = [(0, 1), (1, 0)]
F32 = jnp.float32
BF16 = jnp.bfloat16


def class_of(e):
    return (e ^ (e // 2)) % 2


def swapped(array):
    return lax.ppermute(array, "tp", SWAP)


def iota(shape, dim):
    return lax.broadcasted_iota(jnp.int32, shape, dim)


def mm(a, b):
    return jnp.dot(a, b, preferred_element_type=F32)


def mm_t(a, b):
    return lax.dot_general(a, b, (((1,), (1,)), ((), ())), preferred_element_type=F32)


def silu(v):
    return v / (1.0 + jnp.exp(-v))


def params(limit=56):
    return pltpu.CompilerParams(vmem_limit_bytes=limit << 20)


def whole(shape):
    return pl.BlockSpec(shape, lambda *_: (0,) * len(shape))


def near_call(kernel, arrays, outs, scratch=(), limit=32):
    here = pl.BlockSpec(memory_space=pltpu.VMEM)
    many = isinstance(outs, list)
    return pl.pallas_call(
        kernel,
        in_specs=[here] * len(arrays),
        out_specs=[here] * len(outs) if many else here,
        out_shape=outs,
        scratch_shapes=list(scratch),
        compiler_params=params(limit),
    )(*arrays)


def kept(ref, dim, size, other=False):
    rank = lax.axis_index("tp")
    rank = 1 - rank if other else rank
    at = pl.ds(pl.multiple_of(rank * size, size), size)
    return ref[at, :] if dim == 0 else ref[:, at]


def laid_out(ref):
    rows = ref[...].astype(F32)
    return jnp.concatenate([rows[r : r + 1, :] for r in range(rows.shape[0])], axis=1)


def tiled(vector):
    return vector.reshape(-1, LANES)


def attend_kernel(
    len_ref, fb, qg, kg, tok_f, ng_f, qw_f, kw_f, vw_f, fw_f, key_f, val_f, gate_f, ow_f,
    partial, fk_out, fv_out, cur_out,
    tok, ng, qw, kw, vw, fw, key, val, gate, ow, sems, *, block,
):
    count = tok.shape[0]
    heads = gate.shape[1]
    hd = key.shape[2]
    span = key.shape[3]
    rows = count * heads
    width = heads * hd
    scale = hd ** (-0.5)
    second = lax.axis_index("tp") == 1
    moves = []

    def fetch(far, buf):
        moves.append(pltpu.make_async_copy(far, buf, sems.at[len(moves)]))
        moves[-1].start()
        return moves[-1]

    first = [fetch(f, v) for f, v in ((tok_f, tok), (ng_f, ng))]
    loads = [fetch(f, v) for f, v in ((qw_f, qw), (kw_f, kw), (vw_f, vw), (fw_f, fw))]
    pieces = [pl.ds(at, block) for at in range(0, count, block)]
    key_moves = [fetch(key_f.at[at], key.at[at]) for at in pieces]
    gate_move = fetch(gate_f, gate)
    val_moves = [fetch(val_f.at[at], val.at[at]) for at in pieces]
    out_load = fetch(ow_f, ow)

    for move in first:
        move.wait()
    x = tok[...].astype(F32)
    ms = jnp.mean(x * x, axis=1, keepdims=True)
    normed = (x * lax.rsqrt(ms + EPS) * laid_out(ng)).astype(BF16)
    for move in loads:
        move.wait()
    q = mm(normed, qw[...])
    k = mm(normed, kw[...])
    v = mm(normed, vw[...])
    k = jnp.where(second, k[:, hd:], k[:, :hd])
    v = jnp.where(second, v[:, hd:], v[:, :hd]).astype(BF16)
    k = k * lax.rsqrt(jnp.mean(k * k, axis=1, keepdims=True) + EPS) * kg[...].astype(F32)
    k = k.astype(BF16)
    fk_out[...] = k
    fv_out[...] = v
    spread = jnp.broadcast_to(q[:, None, :], (count, heads, width)).reshape(rows, width)
    mine = iota((rows, width), 1) // hd == iota((rows, width), 0) % heads
    spread = jnp.where(mine, spread, 0.0)
    msq = jnp.sum(spread * spread, axis=1, keepdims=True) / hd
    spread = spread * lax.rsqrt(msq + EPS)
    gain = jnp.concatenate([qg[...].astype(F32)] * heads, axis=1)
    spread = (spread * gain).astype(BF16)
    pick = (iota((width, hd), 0) % hd == iota((width, hd), 1)).astype(BF16)
    queries_f = mm(spread, pick)
    queries = queries_f.astype(BF16)
    k_rows = jnp.broadcast_to(k.astype(F32)[:, None, :], (count, heads, hd)).reshape(rows, hd)
    own_all = jnp.sum(queries_f * k_rows, axis=1, keepdims=True) * scale
    v_rows = jnp.broadcast_to(v.astype(F32)[:, None, :], (count, heads, hd)).reshape(rows, hd)
    local = jnp.where(second, fw[heads:, :].astype(F32), fw[:heads, :].astype(F32)).astype(BF16)
    bias = jnp.where(second, fb[:, heads:], fb[:, :heads])
    lf = jax.nn.log_sigmoid(mm_t(normed, local) + bias)
    lf = jnp.broadcast_to(lf[:, None, :], (count, heads, heads)).reshape(rows, heads)
    lf = jnp.where(iota((rows, heads), 1) == iota((rows, heads), 0) % heads, lf, 0.0)
    lf_all = jnp.sum(lf, axis=1, keepdims=True)

    pos = iota((rows, span), 1)
    spot = iota((rows, heads), 1) == iota((rows, heads), 0) % heads
    length = jnp.concatenate(
        [jnp.full((heads, 1), len_ref[i], jnp.int32) for i in range(count)], axis=0
    )
    scores = []
    for i in range(count):
        if i % block == 0:
            key_moves[i // block].wait()
        scores.append(mm(queries[i * heads : (i + 1) * heads], key[i, 0]))
    scores = jnp.concatenate(scores, axis=0)
    gate_move.wait()
    gates = gate[...].reshape(rows, span)
    previous = jnp.sum(jnp.where(pos == length - 1, gates, 0.0), axis=1, keepdims=True)
    current = previous + lf_all
    logits = jnp.where(pos < length, scores * scale + (current - gates), -jnp.inf)
    top = jnp.maximum(jnp.max(logits, axis=1, keepdims=True), own_all)
    weights = jnp.exp(logits - top)
    own_weight = jnp.exp(own_all - top)
    total = jnp.sum(weights, axis=1, keepdims=True) + own_weight
    probs = (weights / total).astype(BF16)
    own_prob = (own_weight / total).astype(BF16).astype(F32)
    mixed = []
    for i in range(count):
        if i % block == 0:
            val_moves[i // block].wait()
        mixed.append(mm_t(probs[i * heads : (i + 1) * heads], val[i, 0]))
    mixed = jnp.concatenate(mixed, axis=0) + own_prob * v_rows
    cur = jnp.where(spot, current, 0.0).reshape(count, heads, heads)
    cur_out[...] = jnp.sum(cur, axis=1)

    pick = (iota((hd, width), 1) % hd == iota((hd, width), 0)).astype(BF16)
    wide = mm(mixed.astype(BF16), pick)
    wide = jnp.where(mine, wide, 0.0).reshape(count, heads, width)
    flat = jnp.sum(wide, axis=1).astype(BF16)
    out_load.wait()
    partial[...] = mm(flat, ow[...]).astype(BF16)


def attend(lens, tok, ng, qw, kw, vw, fw, fb, qg, kg, key, val, gate, ow):
    count, heads, _ = gate.shape
    hd = key.shape[2]
    width = tok.shape[1]
    block = 8
    big = (tok, ng, qw, kw, vw, fw, key, val, gate, ow)
    far = pl.BlockSpec(memory_space=pltpu.HBM)
    return pl.pallas_call(
        functools.partial(attend_kernel, block=block),
        grid_spec=pltpu.PrefetchScalarGridSpec(
            num_scalar_prefetch=1,
            grid=(1,),
            in_specs=[whole(fb.shape), whole(qg.shape), whole(kg.shape)] + [far] * len(big),
            out_specs=[
                whole((count, width)), whole((count, hd)), whole((count, hd)), whole((count, heads)),
            ],
            scratch_shapes=[pltpu.VMEM(a.shape, a.dtype) for a in big]
            + [
                pltpu.SemaphoreType.DMA((8 + 2 * (count // block),)),
            ],
        ),
        out_shape=[
            jax.ShapeDtypeStruct((count, width), BF16), jax.ShapeDtypeStruct((count, hd), BF16),
            jax.ShapeDtypeStruct((count, hd), BF16), jax.ShapeDtypeStruct((count, heads), F32),
        ],
        compiler_params=params(60),
        name="attend",
    )(lens, fb, qg, kg, *big)


def column(row, size):
    wide = jnp.broadcast_to(row, (size, size))
    return jnp.sum(jnp.where(iota((size, size), 0) == iota((size, size), 1), wide, 0), axis=1, keepdims=True)


def route_kernel(choice, info_out):
    count = choice.shape[1]
    picks = choice[...].astype(F32)
    earlier = iota((count, count), 1) < iota((count, count), 0)
    lane = iota((count, INFO), 1)
    info = jnp.zeros((count, INFO), F32)
    for k in range(SLOTS):
        mine_k = column(picks[k : k + 1, :], count)
        before = jnp.zeros((count, 1), F32)
        for other in range(SLOTS):
            same = jnp.logical_and(mine_k == picks[other : other + 1, :], earlier)
            before += jnp.sum(jnp.where(same, 1.0, 0.0), axis=1, keepdims=True)
        info = jnp.where(lane == k, mine_k * SLOTS + before, info)
    info_out[...] = info


def route(choice):
    out = jax.ShapeDtypeStruct((choice.shape[1], INFO), F32)
    return near_call(route_kernel, (choice,), out, limit=4)


def norm_kernel(tok, mine, theirs, pg, bg, info, copies, resid_out, branch_out):
    count, width = tok.shape
    half = width // 2
    second = lax.axis_index("tp") == 1
    attn = mine[...].astype(F32) + theirs[...].astype(F32)
    resid = (tok[...].astype(F32) + attn).astype(BF16).astype(F32)
    ms = jnp.mean(resid * resid, axis=1, keepdims=True)
    post = (resid * lax.rsqrt(ms + EPS) * laid_out(pg)).astype(BF16).astype(F32)
    line = jnp.concatenate(
        [jnp.where(second, post[:, half:], post[:, :half]), info[...]], axis=1
    ).astype(BF16)
    for peer in range(copies.shape[0]):
        copies[peer] = line
    logit = jnp.sum(post * laid_out(bg), axis=1, keepdims=True)
    branch_out[...] = jnp.broadcast_to(1.0 / (1.0 + jnp.exp(-logit)), (count, LANES))
    resid_out[...] = jnp.where(second, resid[:, half:], resid[:, :half]).astype(BF16)


def normalize(tok, mine, theirs, pg, bg, info, peers):
    count, width = tok.shape
    half = width // 2
    outs = [
        jax.ShapeDtypeStruct((peers, count, half + INFO), BF16),
        jax.ShapeDtypeStruct((count, half), BF16),
        jax.ShapeDtypeStruct((count, LANES), F32),
    ]
    return near_call(norm_kernel, (tok, mine, theirs, pg, bg, info), outs, limit=8)


def pack_kernel(*refs):
    weights, (out, sems) = refs[:-2], refs[-2:]
    half = out.shape[0]
    units = weights[0].shape[1]
    at = pl.ds(pl.multiple_of(lax.axis_index("tp") * half, half), half)
    moves = [
        pltpu.make_async_copy(w.at[at, :], out.at[:, pl.ds(n * units, units)], sems.at[n])
        for n, w in enumerate(weights)
    ]
    for move in moves:
        move.start()
    for move in moves:
        move.wait()


def pack_down_kernel(*refs):
    weights, (out, sems) = refs[:-2], refs[-2:]
    half = out.shape[1]
    units = weights[0].shape[0]
    at = pl.ds(pl.multiple_of(lax.axis_index("tp") * half, half), half)
    moves = [
        pltpu.make_async_copy(w.at[:, at], out.at[pl.ds(n * units, units), :], sems.at[n])
        for n, w in enumerate(weights)
    ]
    for move in moves:
        move.start()
    for move in moves:
        move.wait()


def pack(kernel, weights, shape):
    return pl.pallas_call(
        kernel,
        in_specs=[pl.BlockSpec(memory_space=pltpu.HBM)] * len(weights),
        out_specs=pl.BlockSpec(memory_space=pltpu.VMEM),
        out_shape=jax.ShapeDtypeStruct(shape, BF16),
        scratch_shapes=[pltpu.SemaphoreType.DMA((len(weights),))],
        compiler_params=params(16),
    )(*weights)


def hidden_kernel(x, wide, out):
    half = wide.shape[0]
    tokens = x[:, :half]
    for b in range(wide.shape[1] // 256):
        at = slice(256 * b, 256 * (b + 1))
        out[:, at] = mm(tokens, wide[:, at]).astype(BF16)


def dense_hidden(lines, wide):
    out = jax.ShapeDtypeStruct((lines.shape[0], wide.shape[1]), BF16)
    return near_call(hidden_kernel, (lines, wide), out, limit=16)


def extract_kernel(x, own_rows, near_rows, *, count):
    total = x.shape[0]
    half = own_rows.shape[1]
    peers = total // count
    shape = (total, 4 * peers)
    col = iota((1, 4 * peers), 1)
    expert = lax.axis_index("ep") ^ (col // (2 * peers))
    want = (expert * SLOTS + (col // peers) % 2).astype(F32)
    low = (col % peers) * count
    token = iota(shape, 0)
    info = x[:, half:].astype(F32)
    hit = jnp.logical_or(info[:, 0:1] == want, info[:, 1:2] == want)
    hit = jnp.logical_and(hit, jnp.logical_and(token >= low, token < low + count))
    pick = jnp.where(hit, 1.0, 0.0).astype(BF16)
    rows = lax.dot_general(
        pick, x[:, :half], (((0,), (0,)), ((), ())), preferred_element_type=F32
    ).astype(BF16)
    own_rows[...] = rows[: 2 * peers, :]
    near_rows[...] = rows[2 * peers :, :]


def extract(lines, count):
    total, wide = lines.shape
    rows = jax.ShapeDtypeStruct((2 * total // count, wide - INFO), BF16)
    kernel = functools.partial(extract_kernel, count=count)
    return near_call(kernel, (lines,), [rows, rows], limit=16)


def down_kernel(mine, theirs, down, far, squares_far, out, hid, squares, sems, *, count, block):
    units = mine.shape[1] // 8
    total, _ = out.shape
    peers = total // count
    steps = [slice(at, at + block) for at in range(0, total, block)]
    part = jnp.zeros((peers, LANES), F32)
    for at in steps:

        def full(b):
            there = b ^ 1
            return mine[at, b * units : (b + 1) * units].astype(F32) + theirs[
                at, there * units : (there + 1) * units
            ].astype(F32)

        hidden = [silu(full(b)) * full(b + 2) for b in (0, 1, 4, 5)]
        square = jnp.sum(sum(h * h for h in hidden), axis=1, keepdims=True)
        hid[at, :] = jnp.concatenate([a.astype(BF16) for a in hidden], axis=1)
        token = iota((block, LANES), 0) + at.start
        spread = jnp.where(iota((block, LANES), 1) == token % count, square, 0.0)
        high = spread.astype(BF16)
        low = (spread - high.astype(F32)).astype(BF16)
        here = iota((peers, block), 1) + at.start
        start = iota((peers, block), 0) * count
        owner = jnp.logical_and(here >= start, here < start + count)
        owner = jnp.where(owner, 1.0, 0.0).astype(BF16)
        part += mm(owner, high) + mm(owner, low)
    squares[...] = part
    moves = [pltpu.make_async_copy(squares, squares_far, sems.at[0])]
    moves[0].start()
    for n, at in enumerate(steps):
        out[at, :] = mm(hid[at, :], down[...]).astype(BF16)
        moves.append(pltpu.make_async_copy(out.at[at, :], far.at[at, :], sems.at[n + 1]))
        moves[-1].start()
    for move in moves:
        move.wait()


def dense_down(mine, theirs, down, count):
    total = mine.shape[0]
    units, half = down.shape
    block = 256
    here = pl.BlockSpec(memory_space=pltpu.VMEM)
    far = pl.BlockSpec(memory_space=pltpu.HBM)
    return pl.pallas_call(
        functools.partial(down_kernel, count=count, block=block),
        in_specs=[here] * 3,
        out_specs=[far, far],
        out_shape=[
            jax.ShapeDtypeStruct((total, half), BF16),
            jax.ShapeDtypeStruct((total // count, LANES), F32),
        ],
        scratch_shapes=[
            pltpu.VMEM((total, half), BF16), pltpu.VMEM((total, units), BF16),
            pltpu.VMEM((total // count, LANES), F32),
            pltpu.SemaphoreType.DMA((total // block + 1,)),
        ],
        compiler_params=params(16),
        name="dense_down",
    )(mine, theirs, down)


def expert_kernel(a0, b0, a1, b1, gw, uw, dw, after, keep, give, gbuf, ubuf, dbuf, sems):
    half = a0.shape[1]
    moves = []
    for n, (far, buf) in enumerate(((gw, gbuf), (uw, ubuf), (dw, dbuf))):
        part = buf.shape[0] // 2
        for m in range(2):
            at = pl.ds(m * part, part)
            moves.append(pltpu.make_async_copy(far.at[0, at, :], buf.at[at, :], sems.at[2 * n + m]))
            moves[-1].start()
    x0 = jnp.concatenate([a0[...], b0[...]], axis=0)
    x1 = jnp.concatenate([a1[...], b1[...]], axis=0)

    def rows(w):
        return mm(x0, kept(w, 0, half)) + mm(x1, kept(w, 0, half, True))

    moves[0].wait()
    moves[1].wait()
    gate = silu(rows(gbuf))
    moves[2].wait()
    moves[3].wait()
    act = (gate * rows(ubuf)).astype(BF16)
    moves[4].wait()
    moves[5].wait()
    keep[...] = mm(act, kept(dbuf, 1, half)).astype(BF16)
    give[...] = mm(act, kept(dbuf, 1, half, True)).astype(BF16)


def experts(rows, away, gate_w, up_w, down_w, after):
    count, half = rows[0].shape
    here = pl.BlockSpec(memory_space=pltpu.VMEM)
    far = pl.BlockSpec(memory_space=pltpu.HBM)
    return pl.pallas_call(
        expert_kernel,
        in_specs=[here] * 4 + [far] * 3 + [here],
        out_specs=[here] * 2,
        out_shape=[jax.ShapeDtypeStruct((2 * count, half), BF16)] * 2,
        scratch_shapes=[pltpu.VMEM(w.shape[1:], BF16) for w in (gate_w, up_w, down_w)]
        + [pltpu.SemaphoreType.DMA((6,))],
        compiler_params=params(60),
        name="experts",
    )(*rows, *away, gate_w, up_w, down_w, after)


def merge_kernel(keep, other, near):
    half = near.shape[0]
    near[...] = (keep[half:, :].astype(F32) + other[half:, :].astype(F32)).astype(BF16)


def merge(keep, other):
    out = jax.ShapeDtypeStruct((keep.shape[0] // 2, keep.shape[1]), BF16)
    return near_call(merge_kernel, (keep, other), out, limit=16)


def answer_kernel(keep, other, near, squares, out, scr):
    peers = out.shape[0]
    half = near.shape[0]
    own = keep[:half, :].astype(F32) + other[:half, :].astype(F32)
    parts = own.shape[1] // LANES
    for g, total in enumerate((own, near[...].astype(F32))):
        for s in range(SLOTS):
            for f in range(parts):
                scr[:, parts * (SLOTS * g + s) + f, :] = total[
                    peers * s : peers * (s + 1), LANES * f : LANES * (f + 1)
                ]
    out[:, : 2 * SLOTS * parts, :] = scr[...].astype(BF16)
    out[:, 2 * SLOTS * parts :, :] = jnp.broadcast_to(
        squares[...][:, None, :], (peers, 8, LANES)
    ).astype(BF16)


def answers(keep, other, near, squares):
    peers = squares.shape[0]
    rows = 2 * SLOTS * keep.shape[1] // LANES
    out = jax.ShapeDtypeStruct((peers, rows + 8, LANES), BF16)
    scratch = [pltpu.VMEM((peers, rows, LANES), F32)]
    return near_call(answer_kernel, (keep, other, near, squares), out, scratch, limit=16)


def last_kernel(returned, parts, info, weight, branch, resid, out, scr):
    count, half = resid.shape
    peers = returned.shape[0]
    tiles = half // LANES
    rows = 2 * SLOTS * tiles
    scr[...] = returned[:, :rows, :].astype(F32)
    values = jnp.concatenate(
        [
            jnp.concatenate([scr[:, tiles * b + f, :] for f in range(tiles)], axis=1)
            for b in range(2 * SLOTS)
        ],
        axis=0,
    ).astype(BF16)
    lane = iota((1, 2 * SLOTS * peers), 1)
    peer = lane % peers
    expert = (2 * peer + (peer + class_of(lax.axis_index("ep"))) % 2) ^ (lane // (SLOTS * peers))
    code = (expert * SLOTS + (lane // peers) % SLOTS).astype(F32)
    expert_sum = jnp.zeros((count, half), F32)
    for k in range(SLOTS):
        pick = jnp.where(info[:, k : k + 1] == code, 1.0, 0.0).astype(BF16)
        expert_sum += column(weight[k : k + 1, :], count) * mm(pick, values)
    square = jnp.sum(returned[:, rows : rows + 8, :].astype(F32), axis=0)
    square = column(square[0:1, :count], count)
    dense = jnp.sum(parts[...].astype(F32), axis=0)
    dense = (dense * lax.rsqrt(square / FF2 + EPS)).astype(BF16).astype(F32)
    out[...] = (resid[...].astype(F32) + expert_sum + branch[:, :1] * dense).astype(BF16)


def last_sum(returned, parts, info, weight, branch, resid):
    arrays = (returned, parts, info, weight, branch, resid)
    out = jax.ShapeDtypeStruct(resid.shape, BF16)
    scratch = [pltpu.VMEM((returned.shape[0], 2 * SLOTS * resid.shape[1] // LANES, LANES), F32)]
    return near_call(last_kernel, arrays, out, scratch, limit=16)


def body(
    tokens,
    norm_gain,
    query_w,
    key_w,
    value_w,
    forget_w,
    forget_bias,
    query_gain,
    key_gain,
    cache_key,
    cache_value,
    cache_gate,
    cache_len,
    out_w,
    post_gain,
    branch_gate,
    dense_gate_w,
    dense_up_w,
    dense_down_w,
    expert_choice,
    route_weight,
    expert_gate_w,
    expert_up_w,
    expert_down_w,
):
    count = tokens.shape[0]
    ep_count = lax.axis_size("ep")
    peers = ep_count // 2
    pair = [(e, e ^ 1) for e in range(ep_count)]
    classes = [[e for e in range(ep_count) if class_of(e) == c] for c in range(2)]

    near = []
    for array in (dense_gate_w, dense_up_w, dense_down_w):
        near.append(lax.ppermute(array, "ep", pair))

    partial, fresh_key, fresh_value, current = attend(
        cache_len, tokens, tiled(norm_gain), query_w, key_w, value_w, forget_w.T,
        forget_bias[None], query_gain[None], key_gain[None], cache_key, cache_value,
        cache_gate, out_w,
    )
    partial_other = swapped(partial)
    info = route(expert_choice.T)
    copies, resid, branch = normalize(
        tokens, partial, partial_other, tiled(post_gain), tiled(branch_gate), info, peers
    )
    lines = lax.all_to_all(copies, "ep", 0, 0, tiled=True, axis_index_groups=classes)
    lines = lines.reshape(peers * count, -1)

    gate_up = []
    for gate_w, up_w in ((dense_gate_w, dense_up_w), (near[0], near[1])):
        gate_up += [gate_w, swapped(gate_w), up_w, swapped(up_w)]
    downs = []
    for down_w in (dense_down_w, near[2]):
        downs += [down_w, swapped(down_w)]

    width, units = dense_gate_w.shape
    wide = pack(pack_kernel, gate_up, (width // 2, len(gate_up) * units))
    down = pack(pack_down_kernel, downs, (len(downs) * units, width // 2))
    part = dense_hidden(lines, wide)
    part_other = swapped(part)
    own_rows, near_rows = extract(lines, count)
    pair_rows = lax.ppermute(near_rows, "ep", pair)
    terms, squares = dense_down(part, part_other, down, count)
    parts = lax.all_to_all(
        terms.reshape(peers, count, -1), "ep", 0, 0, tiled=True, axis_index_groups=classes
    )

    away = (swapped(own_rows), swapped(pair_rows))
    keep, give = experts(
        (own_rows, pair_rows), away, expert_gate_w, expert_up_w, expert_down_w, squares
    )
    other = swapped(give)
    back = lax.ppermute(merge(keep, other), "ep", pair)
    answer = answers(keep, other, back, squares)
    returned = lax.all_to_all(answer, "ep", 0, 0, tiled=True, axis_index_groups=classes)
    mixed_out = last_sum(returned, parts, info, route_weight.T, branch, resid)
    return (mixed_out, fresh_key[:, None, :], fresh_value[:, None, :], current)


def solution(mesh):
    placed = (
        P("ep", None),
        P(),
        P(None, "tp"),
        P(),
        P(),
        P(),
        P(),
        P(),
        P(),
        P("ep", "tp", None, None),
        P("ep", "tp", None, None),
        P("ep", "tp", None),
        P("ep"),
        P("tp", None),
        P(),
        P(),
        P(None, ("ep", "tp")),
        P(None, ("ep", "tp")),
        P(("ep", "tp"), None),
        P("ep", None),
        P("ep", None),
        P("ep", None, "tp"),
        P("ep", None, "tp"),
        P("ep", "tp", None),
    )

    return jax.shard_map(
        body,
        mesh=mesh,
        in_specs=placed,
        out_specs=(P("ep", "tp"), P("ep", "tp", None), P("ep", "tp", None), P("ep", "tp")),
        check_vma=False,
    )
```

time: 145 us -> 146 us (level)
  waiting for transfers between devices: 67.2 us -> 74.4 us
  local copies, waits for them, and re-layouts: 10.8 us -> 7.77 us
  blocking collectives: 22.2 us -> 20 us
    pallas_call x2 -> x3, Pallas kernels: 14.9 us -> 9.16 us  [the longest x1 8.34 us: attend(): pl.pallas_call(functools.partial(attend_kernel, block=block), grid_spec=p...]
    ppermute x0 -> x1, waiting for transfers between devices: none -> 5.49 us  [body(): back = lax.ppermute(merge(keep, other), 'ep', pair)]
    pallas_call x1, Pallas kernels: 1.92 us -> 5.11 us  [experts(): pl.pallas_call(expert_kernel, in_specs=[here] * 4 + [far] * 3 + [here], o...]
    unnamed x47 -> x41, local copies, waits for them, and re-layouts: 10.8 us -> 7.77 us
    all_to_all x1, blocking collectives: 22.2 us -> 20 us  [body(): lax.all_to_all(answer, 'ep', 0, 0, tiled=True, axis_index_groups=classes)]
    ppermute x11, waiting for transfers between devices: 2.51 us -> 4.6 us  [swapped(): return lax.ppermute(array, 'tp', SWAP)]
    pallas_call x5 -> x7, Pallas kernels: 4.06 us -> 5.94 us  [near_call(): pl.pallas_call(kernel, in_specs=[here] * len(arrays), out_specs=[here] *...]
  transfers between devices with their start and end apart: 17 -> 18, of which waited for: 7 -> 9; matrix products, arithmetic and copies ran while one was open for 0% -> 0% of each run, Pallas kernels for 2% -> 3%
where the time goes in v1:
time: 146 us
  waiting for transfers between devices  74.4 us (51%)
  Pallas kernels  23.2 us (16%)
  blocking collectives  20 us (14%)
  starting transfers between devices  19.5 us (13%)
  local copies, waits for them, and re-layouts  7.77 us (5%)
    ppermute x3, waiting for transfers between devices, body(): near.append(lax.ppermute(array, 'ep', pair))  36.2 us
    all_to_all x1, waiting for transfers between devices, body(): lax.all_to_all(terms.reshape(peers, count, -1), 'ep', 0, 0, tiled=True, a...  22.8 us
    all_to_all x1, blocking collectives, body(): lax.all_to_all(answer, 'ep', 0, 0, tiled=True, axis_index_groups=classes)  20 us
    all_to_all x1, starting transfers between devices, body(): lax.all_to_all(copies, 'ep', 0, 0, tiled=True, axis_index_groups=classes)  10.6 us
    pallas_call x1, Pallas kernels, attend(): pl.pallas_call(functools.partial(attend_kernel, block=block), grid_spec=p...  8.34 us
    unnamed x41, local copies, waits for them, and re-layouts  7.77 us
    pallas_call x7, Pallas kernels, near_call(): pl.pallas_call(kernel, in_specs=[here] * len(arrays), out_specs=[here] *...  5.94 us
    ppermute x1, waiting for transfers between devices, body(): back = lax.ppermute(merge(keep, other), 'ep', pair)  5.49 us
  transfers between devices with their start and end apart: 18, of which 9 were waited for; matrix products, arithmetic and copies ran while one was open for 0% of the time, Pallas kernels for 3%

profile of v1, /device:TPU:0, one launch (start us, length us, event | category | flops | bytes accessed | tf_op | source)
XLA Modules:
  0.0 145.9 jit_solution(841753270849388449)
XLA Ops:
  0.7 8.3 %attend.1 = (bf16[24,2048]{1,0:T(8,128)(2,1)}, bf16[24,64]{1,0:T(8,128)(2,1)}, bf16[24,64]{1,0:T(8,128)(2,1)}, f32[24,8]{1,0:T(8,128)}) custom-call(s32[24]{0:T(128)} %len_ref.1, f32[1,16]{1,0:T(1,128)} %bitcast.21, bf16[1,64]{1,0:T(2,128)(2,1)} %bitcast.22, bf16[1,64]{1,0:T(2,128)(2,1)} %bitcast.23, bf16[24,2048]{1,0:T(8,128)(2,1)} %tok.1, ...), custom_call_target="tpu_custom_call" | custom-call | tf_op jit(solution)/shard_map/attend/pallas_call | solution.py:192
  9.0 0.0 copy-start.4
  9.0 0.0 copy-start.5
  9.0 0.1 collective-permute-start
  9.1 0.0 copy-done.15
  9.1 0.2 shard_map.255.info
  9.3 1.3 collective-permute-done.theirs
  10.6 0.0 copy-done.13
  10.6 0.0 copy-start.9
  10.7 0.9 copy-done.9
  11.5 1.5 %shard_map.256 = (bf16[32,24,1152]{2,1,0:T(8,128)(2,1)}, bf16[24,1024]{1,0:T(8,128)(2,1)S(1)}, f32[24,128]{1,0:T(8,128)S(1)}) custom-call(bf16[24,2048]{1,0:T(8,128)(2,1)S(1)} %copy-done.7, bf16[24,2048]{1,0:T(8,128)(2,1)S(1)} %copy-done.9, bf16[24,2048]{1,0:T(8,128)(2,1)S(1)} %collective-permute-done.theirs, bf16[16,128]{1,0:T(8,128)(2,1)S(1)} %bitcast.15, ...), custom_call_target="tpu_custom_call" | custom-call | tf_op jit(solution)/shard_map/pallas_call | solution.py:56
  13.0 10.6 %all-to-all-start = ((bf16[32,24,1152]{2,1,0:T(8,128)(2,1)}), bf16[32,24,1152]{2,1,0:T(8,128)(2,1)S(1)}, u32[]{:S(2)}, u32[]{:S(2)}) async-start(bf16[32,24,1152]{2,1,0:T(8,128)(2,1)} %get-tuple-element.18), calls=%async_computation | async-start | bytes 3538944 | tf_op jit(solution)/shard_map/all_to_all | solution.py:572
  23.7 0.3 collective-permute-start.6
  24.0 1.8 %collective-permute-start.8 = (bf16[2048,128]{1,0:T(8,128)(2,1)S(1)}, bf16[2048,128]{1,0:T(8,128)(2,1)S(1)}, u32[]{:S(2)}, u32[]{:S(2)}) collective-permute-start(bf16[2048,128]{1,0:T(8,128)(2,1)S(1)} %copy-done.5), channel_id=1, source_target_pairs={{0,2},{2,0},{4,6},{6,4},{8,10},{10,8},{12,14},{14,12},{16,18},{18,... | collective-permute-start | bytes 1572872 | tf_op jit(solution)/shard_map/ppermute | solution.py:560
  25.8 0.0 collective-permute-start.4
  25.8 0.5 collective-permute-start.5
  26.3 12.3 %collective-permute-done.6.refs_4_ = bf16[2048,128]{1,0:T(8,128)(2,1)S(1)} collective-permute-done((bf16[2048,128]{1,0:T(8,128)(2,1)S(1)}, bf16[2048,128]{1,0:T(8,128)(2,1)S(1)}, u32[]{:S(2)}, u32[]{:S(2)}) %collective-permute-start.6) | collective-permute-done | bytes 524320 | tf_op jit(solution)/shard_map/ppermute | solution.py:560
  38.6 0.0 collective-permute-start.7
  38.6 10.1 %collective-permute-done.8.refs_6_ = bf16[2048,128]{1,0:T(8,128)(2,1)S(1)} collective-permute-done((bf16[2048,128]{1,0:T(8,128)(2,1)S(1)}, bf16[2048,128]{1,0:T(8,128)(2,1)S(1)}, u32[]{:S(2)}, u32[]{:S(2)}) %collective-permute-start.8) | collective-permute-done | bytes 524320 | tf_op jit(solution)/shard_map/ppermute | solution.py:560
  48.7 0.0 collective-permute-start.9
  48.7 0.0 collective-permute-done.4.refs_1_
  48.7 0.0 collective-permute-done.5.refs_3_
  48.7 0.0 collective-permute-done.7.refs_5_
  48.7 1.9 %collective-permute-done.9.refs_7_ = bf16[2048,128]{1,0:T(8,128)(2,1)S(1)} collective-permute-done((bf16[2048,128]{1,0:T(8,128)(2,1)S(1)}, bf16[2048,128]{1,0:T(8,128)(2,1)S(1)}, u32[]{:S(2)}, u32[]{:S(2)}) %collective-permute-start.9) | collective-permute-done | bytes 524320 | tf_op jit(solution)/shard_map/ppermute | solution.py:26
  50.6 0.7 shard_map.258.wide
  51.3 1.3 copy-done
  52.7 0.0 all-to-all-done
  52.7 1.6 %copy-done.1 = bf16[1024,1024]{1,0:T(8,128)(2,1)S(1)} copy-done((bf16[1024,1024]{1,0:T(8,128)(2,1)S(1)}, bf16[1024,1024]{1,0:T(8,128)(2,1)}, u32[]{:S(2)}) %copy-start.1) | copy-done | bytes 2097176
  54.3 1.8 %shard_map.259.mine = bf16[768,1024]{1,0:T(8,128)(2,1)S(1)} custom-call(bf16[768,1152]{1,0:T(8,128)(2,1)S(1)} %bitcast.13, bf16[1024,1024]{1,0:T(8,128)(2,1)S(1)} %copy-done.1), custom_call_target="tpu_custom_call" | custom-call | tf_op jit(solution)/shard_map/pallas_call | solution.py:56
  56.1 0.2 collective-permute-start.10
  56.3 0.3 collective-permute-start.12
  56.6 0.1 collective-permute-start.11
  56.7 13.8 %collective-permute-done.12.refs_2_ = bf16[128,2048]{1,0:T(8,128)(2,1)S(1)} collective-permute-done((bf16[128,2048]{1,0:T(8,128)(2,1)S(1)}, bf16[128,2048]{1,0:T(8,128)(2,1)S(1)}, u32[]{:S(2)}, u32[]{:S(2)}) %collective-permute-start.12) | collective-permute-done | bytes 524320 | tf_op jit(solution)/shard_map/ppermute | solution.py:560
  70.5 0.0 collective-permute-start.13
  70.5 0.6 shard_map.257
  71.1 0.4 collective-permute-start.1
  71.5 0.3 collective-permute-start.2
  71.8 5.3 %collective-permute-done.1.b0 = bf16[64,1024]{1,0:T(8,128)(2,1)S(1)} collective-permute-done((bf16[64,1024]{1,0:T(8,128)(2,1)S(1)}, bf16[64,1024]{1,0:T(8,128)(2,1)S(1)}, u32[]{:S(2)}, u32[]{:S(2)}) %collective-permute-start.1) | collective-permute-done | bytes 131104 | tf_op jit(solution)/shard_map/ppermute | solution.py:588
  77.1 0.0 collective-permute-start.3
  77.1 0.0 collective-permute-done.11.refs_1_
  77.1 0.0 collective-permute-done.13.refs_3_
  77.1 0.1 shard_map.260.down
  77.3 0.0 collective-permute-done.10.theirs
  77.3 3.0 %dense_down.1 = (bf16[768,1024]{1,0:T(8,128)(2,1)}, f32[32,128]{1,0:T(8,128)S(1)}) custom-call(bf16[768,1024]{1,0:T(8,128)(2,1)S(1)} %shard_map.259.mine, bf16[768,1024]{1,0:T(8,128)(2,1)S(1)} %collective-permute-done.10.theirs, bf16[512,1024]{1,0:T(8,128)(2,1)S(1)} %shard_map.260.down), custom_call_target="tpu_custom_call" | custom-call | tf_op jit(solution)/shard_map/dense_down/pallas_call | solution.py:395
  80.3 0.0 copy-start.10
  80.3 0.6 copy-done.10
  80.9 0.0 collective-permute-done.2.a1
  80.9 0.0 collective-permute-done.3.b1
  80.9 0.6 copy-done.17
  81.5 0.1 copy-done.18
  81.6 5.1 %experts.1 = (bf16[128,1024]{1,0:T(8,128)(2,1)}, bf16[128,1024]{1,0:T(8,128)(2,1)}) custom-call(bf16[64,1024]{1,0:T(8,128)(2,1)} %copy-done.8, bf16[64,1024]{1,0:T(8,128)(2,1)} %copy-done.16, bf16[64,1024]{1,0:T(8,128)(2,1)} %copy-done.17, bf16[64,1024]{1,0:T(8,128)(2,1)} %copy-done.18, bf16[1,2048,512]{2,1,0:T(8,128)(2,1)} %gw.1, bf16[1,2048,512]{2,1,0:T(8,128)(2,1)} %uw.1, ...), custom_call_target="tpu_custom_call" | custom-call | tf_op jit(solution)/shard_map/experts/pallas_call | solution.py:444
  86.7 0.6 collective-permute-start.14
  87.3 1.4 collective-permute-done.14.other
  88.7 0.9 copy-done.2
  89.7 0.4 collective-permute-start.15
  90.0 5.5 %collective-permute-done.15.near = bf16[64,1024]{1,0:T(8,128)(2,1)S(1)} collective-permute-done((bf16[64,1024]{1,0:T(8,128)(2,1)S(1)}, bf16[64,1024]{1,0:T(8,128)(2,1)S(1)}, u32[]{:S(2)}, u32[]{:S(2)}) %collective-permute-start.15) | collective-permute-done | bytes 131104 | tf_op jit(solution)/shard_map/ppermute | solution.py:599
  95.5 0.9 copy-done.3
  96.5 0.6 shard_map.262
  97.1 0.0 copy-start.14
  97.1 20.0 %all_to_all.15.returned = bf16[32,40,128]{2,1,0:T(8,128)(2,1)S(1)} all-to-all(bf16[32,40,128]{2,1,0:T(8,128)(2,1)S(1)} %shard_map.262), channel_id=1, replica_groups={{0,6,8,14,16,22,24,30,32,38,40,46,48,54,56,62,64,70,72,78,80,86,88,94,9..., dimensions={0} | all-to-all | bytes 655360 | tf_op jit(solution)/shard_map/all_to_all | solution.py:601
  117.1 4.0 %all-to-all-start.2 = ((bf16[32,24,1024]{2,1,0:T(8,128)(2,1)}), bf16[32,24,1024]{2,1,0:T(8,128)(2,1)S(1)}, u32[]{:S(2)}, u32[]{:S(2)}) async-start(bf16[32,24,1024]{2,1,0:T(8,128)(2,1)} %bitcast.9), calls=%async_computation.2 | async-start | bytes 3145728 | tf_op jit(solution)/shard_map/all_to_all | solution.py:590
  121.1 0.7 copy.28
  121.8 22.8 %all-to-all-done.2.parts = bf16[32,24,1024]{2,1,0:T(8,128)(2,1)S(1)} async-done(((bf16[32,24,1024]{2,1,0:T(8,128)(2,1)}), bf16[32,24,1024]{2,1,0:T(8,128)(2,1)S(1)}, u32[]{:S(2)}, u32[]{:S(2)}) %all-to-all-start.2) | async-done | bytes 1572896 | tf_op jit(solution)/shard_map/all_to_all | solution.py:590
  144.6 1.3 shard_map.263
  (26 shorter events, 0.1 us)
Async XLA Ops:
  0.6 8.5 %copy-start.15 = (s32[24,2]{0,1:T(2,128)S(1)}, s32[24,2]{0,1:T(2,128)}, u32[]{:S(2)}) copy-start(s32[24,2]{0,1:T(2,128)} %param.43) | copy-start | bytes 580
  0.6 10.0 %copy-start.7 = (bf16[24,2048]{1,0:T(8,128)(2,1)S(1)}, bf16[24,2048]{1,0:T(8,128)(2,1)}, u32[]{:S(2)}) copy-start(bf16[24,2048]{1,0:T(8,128)(2,1)} %tok.1) | copy-start | bytes 294916
  0.7 10.0 %copy-start.12 = (bf16[2048]{0:T(1024)(128)(2,1)S(1)}, bf16[2048]{0:T(1024)(128)(2,1)}, u32[]{:S(2)}) copy-start(bf16[2048]{0:T(1024)(128)(2,1)} %param.38) | copy-start | bytes 12292
  0.7 10.0 %copy-start.13 = (bf16[2048]{0:T(1024)(128)(2,1)S(1)}, bf16[2048]{0:T(1024)(128)(2,1)}, u32[]{:S(2)}) copy-start(bf16[2048]{0:T(1024)(128)(2,1)} %param.39) | copy-start | bytes 12292
  9.0 14.7 %copy-start.4 = (bf16[2048,128]{1,0:T(8,128)(2,1)S(1)}, bf16[2048,128]{1,0:T(8,128)(2,1)}, u32[]{:S(2)}) copy-start(bf16[2048,128]{1,0:T(8,128)(2,1)} %refs_0_.2) | copy-start | bytes 1572868
  9.0 15.0 %copy-start.5 = (bf16[2048,128]{1,0:T(8,128)(2,1)S(1)}, bf16[2048,128]{1,0:T(8,128)(2,1)}, u32[]{:S(2)}) copy-start(bf16[2048,128]{1,0:T(8,128)(2,1)} %refs_2_.1) | copy-start | bytes 1572868
  9.0 1.6 %collective-permute-start = (bf16[24,2048]{1,0:T(8,128)(2,1)}, bf16[24,2048]{1,0:T(8,128)(2,1)S(1)}, u32[]{:S(2)}, u32[]{:S(2)}) collective-permute-start(bf16[24,2048]{1,0:T(8,128)(2,1)} %get-tuple-element.17.mine), channel_id=1, source_target_pairs={{0,1},{1,0},{2,3},{3,2},{4,5},{5,4},{6,7},{7,6},{8,9},{9,8},{10,11... | collective-permute-start | bytes 294920 | tf_op jit(solution)/shard_map/ppermute | solution.py:26
  10.6 0.9 copy-start.9
  13.0 39.6 %all-to-all-start = ((bf16[32,24,1152]{2,1,0:T(8,128)(2,1)}), bf16[32,24,1152]{2,1,0:T(8,128)(2,1)S(1)}, u32[]{:S(2)}, u32[]{:S(2)}) async-start(bf16[32,24,1152]{2,1,0:T(8,128)(2,1)} %get-tuple-element.18), calls=%async_computation | async-start | bytes 3538944 | tf_op jit(solution)/shard_map/all_to_all | solution.py:572
  23.7 14.9 %collective-permute-start.6 = (bf16[2048,128]{1,0:T(8,128)(2,1)S(1)}, bf16[2048,128]{1,0:T(8,128)(2,1)S(1)}, u32[]{:S(2)}, u32[]{:S(2)}) collective-permute-start(bf16[2048,128]{1,0:T(8,128)(2,1)S(1)} %copy-done.4), channel_id=1, source_target_pairs={{0,2},{2,0},{4,6},{6,4},{8,10},{10,8},{12,14},{14,12},{16,18},{18,... | collective-permute-start | bytes 1572872 | tf_op jit(solution)/shard_map/ppermute | solution.py:560
  24.0 24.7 %collective-permute-start.8 = (bf16[2048,128]{1,0:T(8,128)(2,1)S(1)}, bf16[2048,128]{1,0:T(8,128)(2,1)S(1)}, u32[]{:S(2)}, u32[]{:S(2)}) collective-permute-start(bf16[2048,128]{1,0:T(8,128)(2,1)S(1)} %copy-done.5), channel_id=1, source_target_pairs={{0,2},{2,0},{4,6},{6,4},{8,10},{10,8},{12,14},{14,12},{16,18},{18,... | collective-permute-start | bytes 1572872 | tf_op jit(solution)/shard_map/ppermute | solution.py:560
  25.8 22.9 %collective-permute-start.4 = (bf16[2048,128]{1,0:T(8,128)(2,1)S(1)}, bf16[2048,128]{1,0:T(8,128)(2,1)S(1)}, u32[]{:S(2)}, u32[]{:S(2)}) collective-permute-start(bf16[2048,128]{1,0:T(8,128)(2,1)S(1)} %copy-done.4), channel_id=1, source_target_pairs={{0,1},{1,0},{2,3},{3,2},{4,5},{5,4},{6,7},{7,6},{8,9},{9,8},{10,11... | collective-permute-start | bytes 1572872 | tf_op jit(solution)/shard_map/ppermute | solution.py:26
  25.8 22.9 %collective-permute-start.5 = (bf16[2048,128]{1,0:T(8,128)(2,1)S(1)}, bf16[2048,128]{1,0:T(8,128)(2,1)S(1)}, u32[]{:S(2)}, u32[]{:S(2)}) collective-permute-start(bf16[2048,128]{1,0:T(8,128)(2,1)S(1)} %copy-done.5), channel_id=1, source_target_pairs={{0,1},{1,0},{2,3},{3,2},{4,5},{5,4},{6,7},{7,6},{8,9},{9,8},{10,11... | collective-permute-start | bytes 1572872 | tf_op jit(solution)/shard_map/ppermute | solution.py:26
  38.6 10.2 %collective-permute-start.7 = (bf16[2048,128]{1,0:T(8,128)(2,1)S(1)}, bf16[2048,128]{1,0:T(8,128)(2,1)S(1)}, u32[]{:S(2)}, u32[]{:S(2)}) collective-permute-start(bf16[2048,128]{1,0:T(8,128)(2,1)S(1)} %collective-permute-done.6.refs_4_), channel_id=1, source_target_pairs={{0,1},{1,0},{2,3},{3,2},{4,5},{5,4},{6,7},{7,6},{8,9},{9,8},{10,11... | collective-permute-start | bytes 1572872 | tf_op jit(solution)/shard_map/ppermute | solution.py:26
  48.7 1.9 %collective-permute-start.9 = (bf16[2048,128]{1,0:T(8,128)(2,1)S(1)}, bf16[2048,128]{1,0:T(8,128)(2,1)S(1)}, u32[]{:S(2)}, u32[]{:S(2)}) collective-permute-start(bf16[2048,128]{1,0:T(8,128)(2,1)S(1)} %collective-permute-done.8.refs_6_), channel_id=1, source_target_pairs={{0,1},{1,0},{2,3},{3,2},{4,5},{5,4},{6,7},{7,6},{8,9},{9,8},{10,11... | collective-permute-start | bytes 1572872 | tf_op jit(solution)/shard_map/ppermute | solution.py:26
  51.3 1.4 copy-start
  52.7 1.6 %copy-start.1 = (bf16[1024,1024]{1,0:T(8,128)(2,1)S(1)}, bf16[1024,1024]{1,0:T(8,128)(2,1)}, u32[]{:S(2)}) copy-start(bf16[1024,1024]{1,0:T(8,128)(2,1)} %copy-done) | copy-start | bytes 6291460
  54.3 2.0 %copy-start.6 = (bf16[128,2048]{1,0:T(8,128)(2,1)S(1)}, bf16[128,2048]{1,0:T(8,128)(2,1)}, u32[]{:S(2)}) copy-start(bf16[128,2048]{1,0:T(8,128)(2,1)} %refs_0_.3) | copy-start | bytes 1572868
  56.1 21.2 %collective-permute-start.10 = (bf16[768,1024]{1,0:T(8,128)(2,1)S(1)}, bf16[768,1024]{1,0:T(8,128)(2,1)S(1)}, u32[]{:S(2)}, u32[]{:S(2)}) collective-permute-start(bf16[768,1024]{1,0:T(8,128)(2,1)S(1)} %shard_map.259.mine), channel_id=1, source_target_pairs={{0,1},{1,0},{2,3},{3,2},{4,5},{5,4},{6,7},{7,6},{8,9},{9,8},{10,11... | collective-permute-start | bytes 4718600 | tf_op jit(solution)/shard_map/ppermute | solution.py:26
  56.3 14.2 %collective-permute-start.12 = (bf16[128,2048]{1,0:T(8,128)(2,1)S(1)}, bf16[128,2048]{1,0:T(8,128)(2,1)S(1)}, u32[]{:S(2)}, u32[]{:S(2)}) collective-permute-start(bf16[128,2048]{1,0:T(8,128)(2,1)S(1)} %copy-done.6), channel_id=1, source_target_pairs={{0,2},{2,0},{4,6},{6,4},{8,10},{10,8},{12,14},{14,12},{16,18},{18,... | collective-permute-start | bytes 1572872 | tf_op jit(solution)/shard_map/ppermute | solution.py:560
  56.6 20.5 %collective-permute-start.11 = (bf16[128,2048]{1,0:T(8,128)(2,1)S(1)}, bf16[128,2048]{1,0:T(8,128)(2,1)S(1)}, u32[]{:S(2)}, u32[]{:S(2)}) collective-permute-start(bf16[128,2048]{1,0:T(8,128)(2,1)S(1)} %copy-done.6), channel_id=1, source_target_pairs={{0,1},{1,0},{2,3},{3,2},{4,5},{5,4},{6,7},{7,6},{8,9},{9,8},{10,11... | collective-permute-start | bytes 1572872 | tf_op jit(solution)/shard_map/ppermute | solution.py:26
  70.5 6.6 %collective-permute-start.13 = (bf16[128,2048]{1,0:T(8,128)(2,1)S(1)}, bf16[128,2048]{1,0:T(8,128)(2,1)S(1)}, u32[]{:S(2)}, u32[]{:S(2)}) collective-permute-start(bf16[128,2048]{1,0:T(8,128)(2,1)S(1)} %collective-permute-done.12.refs_2_), channel_id=1, source_target_pairs={{0,1},{1,0},{2,3},{3,2},{4,5},{5,4},{6,7},{7,6},{8,9},{9,8},{10,11... | collective-permute-start | bytes 1572872 | tf_op jit(solution)/shard_map/ppermute | solution.py:26
  71.1 9.1 %copy-start.8 = (bf16[64,1024]{1,0:T(8,128)(2,1)}, bf16[64,1024]{1,0:T(8,128)(2,1)S(1)}, u32[]{:S(2)}) copy-start(bf16[64,1024]{1,0:T(8,128)(2,1)S(1)} %get-tuple-element.19.a0) | copy-start | bytes 393220
  71.1 6.0 %collective-permute-start.1 = (bf16[64,1024]{1,0:T(8,128)(2,1)S(1)}, bf16[64,1024]{1,0:T(8,128)(2,1)S(1)}, u32[]{:S(2)}, u32[]{:S(2)}) collective-permute-start(bf16[64,1024]{1,0:T(8,128)(2,1)S(1)} %get-tuple-element.20), channel_id=1, source_target_pairs={{0,2},{2,0},{4,6},{6,4},{8,10},{10,8},{12,14},{14,12},{16,18},{18,... | collective-permute-start | bytes 393224 | tf_op jit(solution)/shard_map/ppermute | solution.py:588
  71.5 9.4 %collective-permute-start.2 = (bf16[64,1024]{1,0:T(8,128)(2,1)S(1)}, bf16[64,1024]{1,0:T(8,128)(2,1)S(1)}, u32[]{:S(2)}, u32[]{:S(2)}) collective-permute-start(bf16[64,1024]{1,0:T(8,128)(2,1)S(1)} %get-tuple-element.19.a0), channel_id=1, source_target_pairs={{0,1},{1,0},{2,3},{3,2},{4,5},{5,4},{6,7},{7,6},{8,9},{9,8},{10,11... | collective-permute-start | bytes 393224 | tf_op jit(solution)/shard_map/ppermute | solution.py:26
  77.1 3.2 %copy-start.16 = (bf16[64,1024]{1,0:T(8,128)(2,1)}, bf16[64,1024]{1,0:T(8,128)(2,1)S(1)}, u32[]{:S(2)}) copy-start(bf16[64,1024]{1,0:T(8,128)(2,1)S(1)} %collective-permute-done.1.b0) | copy-start | bytes 393220
  77.1 3.8 %collective-permute-start.3 = (bf16[64,1024]{1,0:T(8,128)(2,1)S(1)}, bf16[64,1024]{1,0:T(8,128)(2,1)S(1)}, u32[]{:S(2)}, u32[]{:S(2)}) collective-permute-start(bf16[64,1024]{1,0:T(8,128)(2,1)S(1)} %collective-permute-done.1.b0), channel_id=1, source_target_pairs={{0,1},{1,0},{2,3},{3,2},{4,5},{5,4},{6,7},{7,6},{8,9},{9,8},{10,11... | collective-permute-start | bytes 393224 | tf_op jit(solution)/shard_map/ppermute | solution.py:26
  80.3 0.6 copy-start.10
  80.9 0.7 copy-start.17
  80.9 0.7 copy-start.18
  81.6 13.9 %copy-start.11 = (f32[32,128]{1,0:T(8,128)S(1)}, f32[32,128]{1,0:T(8,128)}, u32[]{:S(2)}) copy-start(f32[32,128]{1,0:T(8,128)} %copy-done.10) | copy-start | bytes 49156
  86.7 1.9 %collective-permute-start.14 = (bf16[128,1024]{1,0:T(8,128)(2,1)}, bf16[128,1024]{1,0:T(8,128)(2,1)S(1)}, u32[]{:S(2)}, u32[]{:S(2)}) collective-permute-start(bf16[128,1024]{1,0:T(8,128)(2,1)} %get-tuple-element.23), channel_id=1, source_target_pairs={{0,1},{1,0},{2,3},{3,2},{4,5},{5,4},{6,7},{7,6},{8,9},{9,8},{10,11... | collective-permute-start | bytes 786440 | tf_op jit(solution)/shard_map/ppermute | solution.py:26
  88.7 0.9 copy-start.2
  89.7 5.9 %collective-permute-start.15 = (bf16[64,1024]{1,0:T(8,128)(2,1)S(1)}, bf16[64,1024]{1,0:T(8,128)(2,1)S(1)}, u32[]{:S(2)}, u32[]{:S(2)}) collective-permute-start(bf16[64,1024]{1,0:T(8,128)(2,1)S(1)} %shard_map.261), channel_id=1, source_target_pairs={{0,2},{2,0},{4,6},{6,4},{8,10},{10,8},{12,14},{14,12},{16,18},{18,... | collective-permute-start | bytes 393224 | tf_op jit(solution)/shard_map/ppermute | solution.py:599
  95.5 1.0 copy-start.3
  97.1 24.0 %copy-start.19 = (f32[24,8]{1,0:T(8,128)S(1)}, f32[24,8]{1,0:T(8,128)}, u32[]{:S(2)}) copy-start(f32[24,8]{1,0:T(8,128)} %get-tuple-element.33) | copy-start | bytes 2308
  97.1 47.5 %copy-start.14 = (f32[24,2]{0,1:T(2,128)S(1)}, f32[24,2]{0,1:T(2,128)}, u32[]{:S(2)}) copy-start(f32[24,2]{0,1:T(2,128)} %param.44) | copy-start | bytes 580
  117.1 27.5 %all-to-all-start.2 = ((bf16[32,24,1024]{2,1,0:T(8,128)(2,1)}), bf16[32,24,1024]{2,1,0:T(8,128)(2,1)S(1)}, u32[]{:S(2)}, u32[]{:S(2)}) async-start(bf16[32,24,1024]{2,1,0:T(8,128)(2,1)} %bitcast.9), calls=%async_computation.2 | async-start | bytes 3145728 | tf_op jit(solution)/shard_map/all_to_all | solution.py:590

commit v2 on v1

--- a/solution.py
+++ b/solution.py
@@ -12,6 +12,7 @@
 LANES = 128
 INFO = 128
 SLOTS = 2
+PIECES = 8
 EPS = 1e-06
 SWAP = [(0, 1), (1, 0)]
 F32 = jnp.float32
@@ -414,10 +415,12 @@
     half = a0.shape[1]
     moves = []
     for n, (far, buf) in enumerate(((gw, gbuf), (uw, ubuf), (dw, dbuf))):
-        part = buf.shape[0] // 2
-        for m in range(2):
+        part = buf.shape[0] // PIECES
+        for m in range(PIECES):
             at = pl.ds(m * part, part)
-            moves.append(pltpu.make_async_copy(far.at[0, at, :], buf.at[at, :], sems.at[2 * n + m]))
+            moves.append(
+                pltpu.make_async_copy(far.at[0, at, :], buf.at[at, :], sems.at[PIECES * n + m])
+            )
             moves[-1].start()
     x0 = jnp.concatenate([a0[...], b0[...]], axis=0)
     x1 = jnp.concatenate([a1[...], b1[...]], axis=0)
@@ -425,14 +428,14 @@
     def rows(w):
         return mm(x0, kept(w, 0, half)) + mm(x1, kept(w, 0, half, True))
 
-    moves[0].wait()
-    moves[1].wait()
+    for move in moves[:PIECES]:
+        move.wait()
     gate = silu(rows(gbuf))
-    moves[2].wait()
-    moves[3].wait()
+    for move in moves[PIECES : 2 * PIECES]:
+        move.wait()
     act = (gate * rows(ubuf)).astype(BF16)
-    moves[4].wait()
-    moves[5].wait()
+    for move in moves[2 * PIECES :]:
+        move.wait()
     keep[...] = mm(act, kept(dbuf, 1, half)).astype(BF16)
     give[...] = mm(act, kept(dbuf, 1, half, True)).astype(BF16)
 
@@ -447,8 +450,8 @@
         out_specs=[here] * 2,
         out_shape=[jax.ShapeDtypeStruct((2 * count, half), BF16)] * 2,
         scratch_shapes=[pltpu.VMEM(w.shape[1:], BF16) for w in (gate_w, up_w, down_w)]
-        + [pltpu.SemaphoreType.DMA((6,))],
-        compiler_params=params(60),
+        + [pltpu.SemaphoreType.DMA((3 * PIECES,))],
+        compiler_params=params(52),
         name="experts",
     )(*rows, *away, gate_w, up_w, down_w, after)
 
@@ -573,8 +576,8 @@
     lines = lines.reshape(peers * count, -1)
 
     gate_up = []
-    for gate_w, up_w in ((dense_gate_w, dense_up_w), (near[0], near[1])):
-        gate_up += [gate_w, swapped(gate_w), up_w, swapped(up_w)]
+    for array in (dense_gate_w, dense_up_w, near[0], near[1]):
+        gate_up += [array, swapped(array)]
     downs = []
     for down_w in (dense_down_w, near[2]):
         downs += [down_w, swapped(down_w)]

time: 146 us -> 141 us (0.966)
  local copies, waits for them, and re-layouts: 7.77 us -> 4.52 us
  Pallas kernels: 23.2 us -> 21.5 us
    unnamed x41 -> x25, local copies, waits for them, and re-layouts: 7.77 us -> 4.52 us
    pallas_call x1, Pallas kernels: 5.11 us -> 3.43 us  [experts(): pl.pallas_call(expert_kernel, in_specs=[here] * 4 + [far] * 3 + [here], o...]
where the time goes in v2:
time: 141 us
  waiting for transfers between devices  74.2 us (53%)
  Pallas kernels  21.5 us (15%)
  blocking collectives  20 us (14%)
  starting transfers between devices  19.5 us (14%)
  local copies, waits for them, and re-layouts  4.52 us (3%)
    ppermute x3, waiting for transfers between devices, body(): near.append(lax.ppermute(array, 'ep', pair))  36.2 us
    all_to_all x1, waiting for transfers between devices, body(): lax.all_to_all(terms.reshape(peers, count, -1), 'ep', 0, 0, tiled=True, a...  22.8 us
    all_to_all x1, blocking collectives, body(): lax.all_to_all(answer, 'ep', 0, 0, tiled=True, axis_index_groups=classes)  20 us
    all_to_all x1, starting transfers between devices, body(): lax.all_to_all(copies, 'ep', 0, 0, tiled=True, axis_index_groups=classes)  10.6 us
    pallas_call x1, Pallas kernels, attend(): pl.pallas_call(functools.partial(attend_kernel, block=block), grid_spec=p...  8.35 us
    pallas_call x7, Pallas kernels, near_call(): pl.pallas_call(kernel, in_specs=[here] * len(arrays), out_specs=[here] *...  5.96 us
    ppermute x1, waiting for transfers between devices, body(): back = lax.ppermute(merge(keep, other), 'ep', pair)  5.48 us
    ppermute x1, waiting for transfers between devices, body(): pair_rows = lax.ppermute(near_rows, 'ep', pair)  5.31 us
  transfers between devices with their start and end apart: 18, of which 9 were waited for; matrix products, arithmetic and copies ran while one was open for 0% of the time, Pallas kernels for 3%

profile of v2, /device:TPU:0, one launch (start us, length us, event | category | flops | bytes accessed | tf_op | source)
XLA Modules:
  0.0 140.7 jit_solution(14673197214215914657)
XLA Ops:
  0.6 0.0 copy-start.10
  0.6 0.0 copy-start.5
  0.7 0.0 copy-start.7
  0.7 0.0 copy-start.8
  0.7 8.3 %attend.1 = (bf16[24,2048]{1,0:T(8,128)(2,1)}, bf16[24,64]{1,0:T(8,128)(2,1)}, bf16[24,64]{1,0:T(8,128)(2,1)}, f32[24,8]{1,0:T(8,128)}) custom-call(s32[24]{0:T(128)} %len_ref.1, f32[1,16]{1,0:T(1,128)} %bitcast.21, bf16[1,64]{1,0:T(2,128)(2,1)} %bitcast.22, bf16[1,64]{1,0:T(2,128)(2,1)} %bitcast.23, bf16[24,2048]{1,0:T(8,128)(2,1)} %tok.1, ...), custom_call_target="tpu_custom_call" | custom-call | tf_op jit(solution)/shard_map/attend/pallas_call | solution.py:193
  9.0 0.0 copy-start.2
  9.0 0.0 copy-start.3
  9.1 0.1 collective-permute-start
  9.1 0.0 copy-done.10
  9.2 0.2 shard_map.255.info
  9.3 1.3 collective-permute-done.theirs
  10.7 0.0 copy-done.8
  10.7 0.0 copy-start.6
  10.7 0.9 copy-done.6
  11.6 1.5 %shard_map.256 = (bf16[32,24,1152]{2,1,0:T(8,128)(2,1)}, bf16[24,1024]{1,0:T(8,128)(2,1)S(1)}, f32[24,128]{1,0:T(8,128)S(1)}) custom-call(bf16[24,2048]{1,0:T(8,128)(2,1)S(1)} %copy-done.5, bf16[24,2048]{1,0:T(8,128)(2,1)S(1)} %copy-done.6, bf16[24,2048]{1,0:T(8,128)(2,1)S(1)} %collective-permute-done.theirs, bf16[16,128]{1,0:T(8,128)(2,1)S(1)} %bitcast.15, ...), custom_call_target="tpu_custom_call" | custom-call | tf_op jit(solution)/shard_map/pallas_call | solution.py:57
  13.1 10.6 %all-to-all-start = ((bf16[32,24,1152]{2,1,0:T(8,128)(2,1)}), bf16[32,24,1152]{2,1,0:T(8,128)(2,1)S(1)}, u32[]{:S(2)}, u32[]{:S(2)}) async-start(bf16[32,24,1152]{2,1,0:T(8,128)(2,1)} %get-tuple-element.18), calls=%async_computation | async-start | bytes 3538944 | tf_op jit(solution)/shard_map/all_to_all | solution.py:575
  23.7 0.0 copy-done.2
  23.7 0.3 collective-permute-start.6
  24.0 1.8 %collective-permute-start.8 = (bf16[2048,128]{1,0:T(8,128)(2,1)S(1)}, bf16[2048,128]{1,0:T(8,128)(2,1)S(1)}, u32[]{:S(2)}, u32[]{:S(2)}) collective-permute-start(bf16[2048,128]{1,0:T(8,128)(2,1)S(1)} %copy-done.3), channel_id=1, source_target_pairs={{0,2},{2,0},{4,6},{6,4},{8,10},{10,8},{12,14},{14,12},{16,18},{18,... | collective-permute-start | bytes 1572872 | tf_op jit(solution)/shard_map/ppermute | solution.py:563
  25.8 0.0 collective-permute-start.4
  25.8 0.5 collective-permute-start.5
  26.3 12.3 %collective-permute-done.6.refs_4_ = bf16[2048,128]{1,0:T(8,128)(2,1)S(1)} collective-permute-done((bf16[2048,128]{1,0:T(8,128)(2,1)S(1)}, bf16[2048,128]{1,0:T(8,128)(2,1)S(1)}, u32[]{:S(2)}, u32[]{:S(2)}) %collective-permute-start.6) | collective-permute-done | bytes 524320 | tf_op jit(solution)/shard_map/ppermute | solution.py:563
  38.6 0.0 collective-permute-start.7
  38.6 10.1 %collective-permute-done.8.refs_6_ = bf16[2048,128]{1,0:T(8,128)(2,1)S(1)} collective-permute-done((bf16[2048,128]{1,0:T(8,128)(2,1)S(1)}, bf16[2048,128]{1,0:T(8,128)(2,1)S(1)}, u32[]{:S(2)}, u32[]{:S(2)}) %collective-permute-start.8) | collective-permute-done | bytes 524320 | tf_op jit(solution)/shard_map/ppermute | solution.py:563
  48.7 0.0 collective-permute-start.9
  48.7 0.0 collective-permute-done.4.refs_1_
  48.7 0.0 collective-permute-done.5.refs_3_
  48.7 0.0 collective-permute-done.7.refs_5_
  48.8 1.9 %collective-permute-done.9.refs_7_ = bf16[2048,128]{1,0:T(8,128)(2,1)S(1)} collective-permute-done((bf16[2048,128]{1,0:T(8,128)(2,1)S(1)}, bf16[2048,128]{1,0:T(8,128)(2,1)S(1)}, u32[]{:S(2)}, u32[]{:S(2)}) %collective-permute-start.9) | collective-permute-done | bytes 524320 | tf_op jit(solution)/shard_map/ppermute | solution.py:27
  50.6 0.7 shard_map.258.wide
  51.4 1.3 copy-done
  52.7 0.0 all-to-all-done
  52.7 1.6 %copy-done.1 = bf16[1024,1024]{1,0:T(8,128)(2,1)S(1)} copy-done((bf16[1024,1024]{1,0:T(8,128)(2,1)S(1)}, bf16[1024,1024]{1,0:T(8,128)(2,1)}, u32[]{:S(2)}) %copy-start.1) | copy-done | bytes 2097176
  54.3 1.8 %shard_map.259.mine = bf16[768,1024]{1,0:T(8,128)(2,1)S(1)} custom-call(bf16[768,1152]{1,0:T(8,128)(2,1)S(1)} %bitcast.13, bf16[1024,1024]{1,0:T(8,128)(2,1)S(1)} %copy-done.1), custom_call_target="tpu_custom_call" | custom-call | tf_op jit(solution)/shard_map/pallas_call | solution.py:57
  56.1 0.2 collective-permute-start.10
  56.3 0.3 collective-permute-start.12
  56.6 0.1 collective-permute-start.11
  56.7 13.8 %collective-permute-done.12.refs_2_ = bf16[128,2048]{1,0:T(8,128)(2,1)S(1)} collective-permute-done((bf16[128,2048]{1,0:T(8,128)(2,1)S(1)}, bf16[128,2048]{1,0:T(8,128)(2,1)S(1)}, u32[]{:S(2)}, u32[]{:S(2)}) %collective-permute-start.12) | collective-permute-done | bytes 524320 | tf_op jit(solution)/shard_map/ppermute | solution.py:563
  70.5 0.0 collective-permute-start.13
  70.5 0.6 shard_map.257
  71.1 0.4 collective-permute-start.1
  71.5 0.3 collective-permute-start.2
  71.8 5.3 %collective-permute-done.1.b0 = bf16[64,1024]{1,0:T(8,128)(2,1)S(1)} collective-permute-done((bf16[64,1024]{1,0:T(8,128)(2,1)S(1)}, bf16[64,1024]{1,0:T(8,128)(2,1)S(1)}, u32[]{:S(2)}, u32[]{:S(2)}) %collective-permute-start.1) | collective-permute-done | bytes 131104 | tf_op jit(solution)/shard_map/ppermute | solution.py:591
  77.1 0.0 collective-permute-start.3
  77.1 0.0 collective-permute-done.11.refs_1_
  77.1 0.0 collective-permute-done.13.refs_3_
  77.1 0.1 shard_map.260.down
  77.3 0.0 collective-permute-done.10.theirs
  77.3 2.9 %dense_down.1 = (bf16[768,1024]{1,0:T(8,128)(2,1)}, f32[32,128]{1,0:T(8,128)S(1)}) custom-call(bf16[768,1024]{1,0:T(8,128)(2,1)S(1)} %shard_map.259.mine, bf16[768,1024]{1,0:T(8,128)(2,1)S(1)} %collective-permute-done.10.theirs, bf16[512,1024]{1,0:T(8,128)(2,1)S(1)} %shard_map.260.down), custom_call_target="tpu_custom_call" | custom-call | tf_op jit(solution)/shard_map/dense_down/pallas_call | solution.py:396
  80.2 0.0 collective-permute-done.2.a1
  80.2 0.0 collective-permute-done.3.b1
  80.2 3.4 %experts.1 = (bf16[128,1024]{1,0:T(8,128)(2,1)S(1)}, bf16[128,1024]{1,0:T(8,128)(2,1)S(1)}) custom-call(bf16[64,1024]{1,0:T(8,128)(2,1)S(1)} %get-tuple-element.19.a0, bf16[64,1024]{1,0:T(8,128)(2,1)S(1)} %collective-permute-done.1.b0, bf16[64,1024]{1,0:T(8,128)(2,1)S(1)} %collective-permute-done.2.a1, bf16[64,1024]{1,0:T(8,128)(2,1)S(1)} %collective-permute-done.3.b1, ...), custom_call_target="tpu_custom_call" | custom-call | tf_op jit(solution)/shard_map/experts/pallas_call | solution.py:447
  83.7 0.6 collective-permute-start.14
  84.2 1.2 collective-permute-done.14.other
  85.4 0.4 collective-permute-start.15
  85.8 5.5 %collective-permute-done.15.near = bf16[64,1024]{1,0:T(8,128)(2,1)S(1)} collective-permute-done((bf16[64,1024]{1,0:T(8,128)(2,1)S(1)}, bf16[64,1024]{1,0:T(8,128)(2,1)S(1)}, u32[]{:S(2)}, u32[]{:S(2)}) %collective-permute-start.15) | collective-permute-done | bytes 131104 | tf_op jit(solution)/shard_map/ppermute | solution.py:602
  91.3 0.6 shard_map.262
  91.9 0.0 copy-start.11
  91.9 0.0 copy-start.9
  91.9 20.0 %all_to_all.15.returned = bf16[32,40,128]{2,1,0:T(8,128)(2,1)S(1)} all-to-all(bf16[32,40,128]{2,1,0:T(8,128)(2,1)S(1)} %shard_map.262), channel_id=1, replica_groups={{0,6,8,14,16,22,24,30,32,38,40,46,48,54,56,62,64,70,72,78,80,86,88,94,9..., dimensions={0} | all-to-all | bytes 655360 | tf_op jit(solution)/shard_map/all_to_all | solution.py:604
  111.9 4.0 %all-to-all-start.2 = ((bf16[32,24,1024]{2,1,0:T(8,128)(2,1)}), bf16[32,24,1024]{2,1,0:T(8,128)(2,1)S(1)}, u32[]{:S(2)}, u32[]{:S(2)}) async-start(bf16[32,24,1024]{2,1,0:T(8,128)(2,1)} %bitcast.9), calls=%async_computation.2 | async-start | bytes 3145728 | tf_op jit(solution)/shard_map/all_to_all | solution.py:593
  115.9 0.7 copy.28
  116.6 22.8 %all-to-all-done.2.parts = bf16[32,24,1024]{2,1,0:T(8,128)(2,1)S(1)} async-done(((bf16[32,24,1024]{2,1,0:T(8,128)(2,1)}), bf16[32,24,1024]{2,1,0:T(8,128)(2,1)S(1)}, u32[]{:S(2)}, u32[]{:S(2)}) %all-to-all-start.2) | async-done | bytes 1572896 | tf_op jit(solution)/shard_map/all_to_all | solution.py:593
  139.4 1.3 shard_map.263
  (10 shorter events, 0.1 us)
Async XLA Ops:
  0.6 8.5 %copy-start.10 = (s32[24,2]{0,1:T(2,128)S(1)}, s32[24,2]{0,1:T(2,128)}, u32[]{:S(2)}) copy-start(s32[24,2]{0,1:T(2,128)} %param.43) | copy-start | bytes 580
  0.6 10.0 %copy-start.5 = (bf16[24,2048]{1,0:T(8,128)(2,1)S(1)}, bf16[24,2048]{1,0:T(8,128)(2,1)}, u32[]{:S(2)}) copy-start(bf16[24,2048]{1,0:T(8,128)(2,1)} %tok.1) | copy-start | bytes 294916
  0.7 10.0 %copy-start.7 = (bf16[2048]{0:T(1024)(128)(2,1)S(1)}, bf16[2048]{0:T(1024)(128)(2,1)}, u32[]{:S(2)}) copy-start(bf16[2048]{0:T(1024)(128)(2,1)} %param.38) | copy-start | bytes 12292
  0.7 10.0 %copy-start.8 = (bf16[2048]{0:T(1024)(128)(2,1)S(1)}, bf16[2048]{0:T(1024)(128)(2,1)}, u32[]{:S(2)}) copy-start(bf16[2048]{0:T(1024)(128)(2,1)} %param.39) | copy-start | bytes 12292
  9.0 14.7 %copy-start.2 = (bf16[2048,128]{1,0:T(8,128)(2,1)S(1)}, bf16[2048,128]{1,0:T(8,128)(2,1)}, u32[]{:S(2)}) copy-start(bf16[2048,128]{1,0:T(8,128)(2,1)} %refs_0_.2) | copy-start | bytes 1572868
  9.0 15.0 %copy-start.3 = (bf16[2048,128]{1,0:T(8,128)(2,1)S(1)}, bf16[2048,128]{1,0:T(8,128)(2,1)}, u32[]{:S(2)}) copy-start(bf16[2048,128]{1,0:T(8,128)(2,1)} %refs_2_.1) | copy-start | bytes 1572868
  9.1 1.6 %collective-permute-start = (bf16[24,2048]{1,0:T(8,128)(2,1)}, bf16[24,2048]{1,0:T(8,128)(2,1)S(1)}, u32[]{:S(2)}, u32[]{:S(2)}) collective-permute-start(bf16[24,2048]{1,0:T(8,128)(2,1)} %get-tuple-element.17.mine), channel_id=1, source_target_pairs={{0,1},{1,0},{2,3},{3,2},{4,5},{5,4},{6,7},{7,6},{8,9},{9,8},{10,11... | collective-permute-start | bytes 294920 | tf_op jit(solution)/shard_map/ppermute | solution.py:27
  10.7 0.9 copy-start.6
  13.1 39.6 %all-to-all-start = ((bf16[32,24,1152]{2,1,0:T(8,128)(2,1)}), bf16[32,24,1152]{2,1,0:T(8,128)(2,1)S(1)}, u32[]{:S(2)}, u32[]{:S(2)}) async-start(bf16[32,24,1152]{2,1,0:T(8,128)(2,1)} %get-tuple-element.18), calls=%async_computation | async-start | bytes 3538944 | tf_op jit(solution)/shard_map/all_to_all | solution.py:575
  23.7 14.9 %collective-permute-start.6 = (bf16[2048,128]{1,0:T(8,128)(2,1)S(1)}, bf16[2048,128]{1,0:T(8,128)(2,1)S(1)}, u32[]{:S(2)}, u32[]{:S(2)}) collective-permute-start(bf16[2048,128]{1,0:T(8,128)(2,1)S(1)} %copy-done.2), channel_id=1, source_target_pairs={{0,2},{2,0},{4,6},{6,4},{8,10},{10,8},{12,14},{14,12},{16,18},{18,... | collective-permute-start | bytes 1572872 | tf_op jit(solution)/shard_map/ppermute | solution.py:563
  24.0 24.7 %collective-permute-start.8 = (bf16[2048,128]{1,0:T(8,128)(2,1)S(1)}, bf16[2048,128]{1,0:T(8,128)(2,1)S(1)}, u32[]{:S(2)}, u32[]{:S(2)}) collective-permute-start(bf16[2048,128]{1,0:T(8,128)(2,1)S(1)} %copy-done.3), channel_id=1, source_target_pairs={{0,2},{2,0},{4,6},{6,4},{8,10},{10,8},{12,14},{14,12},{16,18},{18,... | collective-permute-start | bytes 1572872 | tf_op jit(solution)/shard_map/ppermute | solution.py:563
  25.8 22.9 %collective-permute-start.4 = (bf16[2048,128]{1,0:T(8,128)(2,1)S(1)}, bf16[2048,128]{1,0:T(8,128)(2,1)S(1)}, u32[]{:S(2)}, u32[]{:S(2)}) collective-permute-start(bf16[2048,128]{1,0:T(8,128)(2,1)S(1)} %copy-done.2), channel_id=1, source_target_pairs={{0,1},{1,0},{2,3},{3,2},{4,5},{5,4},{6,7},{7,6},{8,9},{9,8},{10,11... | collective-permute-start | bytes 1572872 | tf_op jit(solution)/shard_map/ppermute | solution.py:27
  25.8 22.9 %collective-permute-start.5 = (bf16[2048,128]{1,0:T(8,128)(2,1)S(1)}, bf16[2048,128]{1,0:T(8,128)(2,1)S(1)}, u32[]{:S(2)}, u32[]{:S(2)}) collective-permute-start(bf16[2048,128]{1,0:T(8,128)(2,1)S(1)} %copy-done.3), channel_id=1, source_target_pairs={{0,1},{1,0},{2,3},{3,2},{4,5},{5,4},{6,7},{7,6},{8,9},{9,8},{10,11... | collective-permute-start | bytes 1572872 | tf_op jit(solution)/shard_map/ppermute | solution.py:27
  38.6 10.2 %collective-permute-start.7 = (bf16[2048,128]{1,0:T(8,128)(2,1)S(1)}, bf16[2048,128]{1,0:T(8,128)(2,1)S(1)}, u32[]{:S(2)}, u32[]{:S(2)}) collective-permute-start(bf16[2048,128]{1,0:T(8,128)(2,1)S(1)} %collective-permute-done.6.refs_4_), channel_id=1, source_target_pairs={{0,1},{1,0},{2,3},{3,2},{4,5},{5,4},{6,7},{7,6},{8,9},{9,8},{10,11... | collective-permute-start | bytes 1572872 | tf_op jit(solution)/shard_map/ppermute | solution.py:27
  48.7 1.9 %collective-permute-start.9 = (bf16[2048,128]{1,0:T(8,128)(2,1)S(1)}, bf16[2048,128]{1,0:T(8,128)(2,1)S(1)}, u32[]{:S(2)}, u32[]{:S(2)}) collective-permute-start(bf16[2048,128]{1,0:T(8,128)(2,1)S(1)} %collective-permute-done.8.refs_6_), channel_id=1, source_target_pairs={{0,1},{1,0},{2,3},{3,2},{4,5},{5,4},{6,7},{7,6},{8,9},{9,8},{10,11... | collective-permute-start | bytes 1572872 | tf_op jit(solution)/shard_map/ppermute | solution.py:27
  51.3 1.3 copy-start
  52.7 1.6 %copy-start.1 = (bf16[1024,1024]{1,0:T(8,128)(2,1)S(1)}, bf16[1024,1024]{1,0:T(8,128)(2,1)}, u32[]{:S(2)}) copy-start(bf16[1024,1024]{1,0:T(8,128)(2,1)} %copy-done) | copy-start | bytes 6291460
  54.3 2.0 %copy-start.4 = (bf16[128,2048]{1,0:T(8,128)(2,1)S(1)}, bf16[128,2048]{1,0:T(8,128)(2,1)}, u32[]{:S(2)}) copy-start(bf16[128,2048]{1,0:T(8,128)(2,1)} %refs_0_.3) | copy-start | bytes 1572868
  56.1 21.2 %collective-permute-start.10 = (bf16[768,1024]{1,0:T(8,128)(2,1)S(1)}, bf16[768,1024]{1,0:T(8,128)(2,1)S(1)}, u32[]{:S(2)}, u32[]{:S(2)}) collective-permute-start(bf16[768,1024]{1,0:T(8,128)(2,1)S(1)} %shard_map.259.mine), channel_id=1, source_target_pairs={{0,1},{1,0},{2,3},{3,2},{4,5},{5,4},{6,7},{7,6},{8,9},{9,8},{10,11... | collective-permute-start | bytes 4718600 | tf_op jit(solution)/shard_map/ppermute | solution.py:27
  56.3 14.2 %collective-permute-start.12 = (bf16[128,2048]{1,0:T(8,128)(2,1)S(1)}, bf16[128,2048]{1,0:T(8,128)(2,1)S(1)}, u32[]{:S(2)}, u32[]{:S(2)}) collective-permute-start(bf16[128,2048]{1,0:T(8,128)(2,1)S(1)} %copy-done.4), channel_id=1, source_target_pairs={{0,2},{2,0},{4,6},{6,4},{8,10},{10,8},{12,14},{14,12},{16,18},{18,... | collective-permute-start | bytes 1572872 | tf_op jit(solution)/shard_map/ppermute | solution.py:563
  56.6 20.5 %collective-permute-start.11 = (bf16[128,2048]{1,0:T(8,128)(2,1)S(1)}, bf16[128,2048]{1,0:T(8,128)(2,1)S(1)}, u32[]{:S(2)}, u32[]{:S(2)}) collective-permute-start(bf16[128,2048]{1,0:T(8,128)(2,1)S(1)} %copy-done.4), channel_id=1, source_target_pairs={{0,1},{1,0},{2,3},{3,2},{4,5},{5,4},{6,7},{7,6},{8,9},{9,8},{10,11... | collective-permute-start | bytes 1572872 | tf_op jit(solution)/shard_map/ppermute | solution.py:27
  70.5 6.6 %collective-permute-start.13 = (bf16[128,2048]{1,0:T(8,128)(2,1)S(1)}, bf16[128,2048]{1,0:T(8,128)(2,1)S(1)}, u32[]{:S(2)}, u32[]{:S(2)}) collective-permute-start(bf16[128,2048]{1,0:T(8,128)(2,1)S(1)} %collective-permute-done.12.refs_2_), channel_id=1, source_target_pairs={{0,1},{1,0},{2,3},{3,2},{4,5},{5,4},{6,7},{7,6},{8,9},{9,8},{10,11... | collective-permute-start | bytes 1572872 | tf_op jit(solution)/shard_map/ppermute | solution.py:27
  71.1 6.0 %collective-permute-start.1 = (bf16[64,1024]{1,0:T(8,128)(2,1)S(1)}, bf16[64,1024]{1,0:T(8,128)(2,1)S(1)}, u32[]{:S(2)}, u32[]{:S(2)}) collective-permute-start(bf16[64,1024]{1,0:T(8,128)(2,1)S(1)} %get-tuple-element.20), channel_id=1, source_target_pairs={{0,2},{2,0},{4,6},{6,4},{8,10},{10,8},{12,14},{14,12},{16,18},{18,... | collective-permute-start | bytes 393224 | tf_op jit(solution)/shard_map/ppermute | solution.py:591
  71.5 8.7 %collective-permute-start.2 = (bf16[64,1024]{1,0:T(8,128)(2,1)S(1)}, bf16[64,1024]{1,0:T(8,128)(2,1)S(1)}, u32[]{:S(2)}, u32[]{:S(2)}) collective-permute-start(bf16[64,1024]{1,0:T(8,128)(2,1)S(1)} %get-tuple-element.19.a0), channel_id=1, source_target_pairs={{0,1},{1,0},{2,3},{3,2},{4,5},{5,4},{6,7},{7,6},{8,9},{9,8},{10,11... | collective-permute-start | bytes 393224 | tf_op jit(solution)/shard_map/ppermute | solution.py:27
  77.1 3.1 %collective-permute-start.3 = (bf16[64,1024]{1,0:T(8,128)(2,1)S(1)}, bf16[64,1024]{1,0:T(8,128)(2,1)S(1)}, u32[]{:S(2)}, u32[]{:S(2)}) collective-permute-start(bf16[64,1024]{1,0:T(8,128)(2,1)S(1)} %collective-permute-done.1.b0), channel_id=1, source_target_pairs={{0,1},{1,0},{2,3},{3,2},{4,5},{5,4},{6,7},{7,6},{8,9},{9,8},{10,11... | collective-permute-start | bytes 393224 | tf_op jit(solution)/shard_map/ppermute | solution.py:27
  83.7 1.7 %collective-permute-start.14 = (bf16[128,1024]{1,0:T(8,128)(2,1)S(1)}, bf16[128,1024]{1,0:T(8,128)(2,1)S(1)}, u32[]{:S(2)}, u32[]{:S(2)}) collective-permute-start(bf16[128,1024]{1,0:T(8,128)(2,1)S(1)} %get-tuple-element.23), channel_id=1, source_target_pairs={{0,1},{1,0},{2,3},{3,2},{4,5},{5,4},{6,7},{7,6},{8,9},{9,8},{10,11... | collective-permute-start | bytes 786440 | tf_op jit(solution)/shard_map/ppermute | solution.py:27
  85.4 5.9 %collective-permute-start.15 = (bf16[64,1024]{1,0:T(8,128)(2,1)S(1)}, bf16[64,1024]{1,0:T(8,128)(2,1)S(1)}, u32[]{:S(2)}, u32[]{:S(2)}) collective-permute-start(bf16[64,1024]{1,0:T(8,128)(2,1)S(1)} %shard_map.261), channel_id=1, source_target_pairs={{0,2},{2,0},{4,6},{6,4},{8,10},{10,8},{12,14},{14,12},{16,18},{18,... | collective-permute-start | bytes 393224 | tf_op jit(solution)/shard_map/ppermute | solution.py:602
  91.9 24.0 %copy-start.11 = (f32[24,8]{1,0:T(8,128)S(1)}, f32[24,8]{1,0:T(8,128)}, u32[]{:S(2)}) copy-start(f32[24,8]{1,0:T(8,128)} %get-tuple-element.33) | copy-start | bytes 2308
  91.9 47.5 %copy-start.9 = (f32[24,2]{0,1:T(2,128)S(1)}, f32[24,2]{0,1:T(2,128)}, u32[]{:S(2)}) copy-start(f32[24,2]{0,1:T(2,128)} %param.44) | copy-start | bytes 580
  111.9 27.5 %all-to-all-start.2 = ((bf16[32,24,1024]{2,1,0:T(8,128)(2,1)}), bf16[32,24,1024]{2,1,0:T(8,128)(2,1)S(1)}, u32[]{:S(2)}, u32[]{:S(2)}) async-start(bf16[32,24,1024]{2,1,0:T(8,128)(2,1)} %bitcast.9), calls=%async_computation.2 | async-start | bytes 3145728 | tf_op jit(solution)/shard_map/all_to_all | solution.py:593

commit v3 on v2

--- a/solution.py
+++ b/solution.py
@@ -309,17 +309,17 @@
     )(*weights)
 
 
-def hidden_kernel(x, wide, out):
-    half = wide.shape[0]
+def hidden_kernel(x, own, far, out):
+    half, cols = own.shape
     tokens = x[:, :half]
-    for b in range(wide.shape[1] // 256):
-        at = slice(256 * b, 256 * (b + 1))
-        out[:, at] = mm(tokens, wide[:, at]).astype(BF16)
-
-
-def dense_hidden(lines, wide):
-    out = jax.ShapeDtypeStruct((lines.shape[0], wide.shape[1]), BF16)
-    return near_call(hidden_kernel, (lines, wide), out, limit=16)
+    for n, wide in enumerate((own, far)):
+        for b in range(0, cols, 256):
+            out[:, n * cols + b : n * cols + b + 256] = mm(tokens, wide[:, b : b + 256]).astype(BF16)
+
+
+def dense_hidden(lines, own, far):
+    out = jax.ShapeDtypeStruct((lines.shape[0], 2 * own.shape[1]), BF16)
+    return near_call(hidden_kernel, (lines, own, far), out, limit=16)
 
 
 def extract_kernel(x, own_rows, near_rows, *, count):
@@ -583,9 +583,10 @@
         downs += [down_w, swapped(down_w)]
 
     width, units = dense_gate_w.shape
-    wide = pack(pack_kernel, gate_up, (width // 2, len(gate_up) * units))
+    far_wide = pack(pack_kernel, gate_up[4:], (width // 2, 4 * units))
+    own_wide = pack(pack_kernel, gate_up[:4], (width // 2, 4 * units))
     down = pack(pack_down_kernel, downs, (len(downs) * units, width // 2))
-    part = dense_hidden(lines, wide)
+    part = dense_hidden(lines, own_wide, far_wide)
     part_other = swapped(part)
     own_rows, near_rows = extract(lines, count)
     pair_rows = lax.ppermute(near_rows, "ep", pair)

time: 141 us -> 140 us (level)
    unnamed x25 -> x27, local copies, waits for them, and re-layouts: 4.52 us -> 4.81 us
where the time goes in v3:
time: 140 us; the launch traced here: 139 us
  waiting for transfers between devices  72.9 us (52%)
  Pallas kernels  21.3 us (15%)
  blocking collectives  20 us (14%)
  starting transfers between devices  19.5 us (14%)
  local copies, waits for them, and re-layouts  4.81 us (3%)
    ppermute x3, waiting for transfers between devices, body(): near.append(lax.ppermute(array, 'ep', pair))  36.2 us
    all_to_all x1, waiting for transfers between devices, body(): lax.all_to_all(terms.reshape(peers, count, -1), 'ep', 0, 0, tiled=True, a...  22.8 us
    all_to_all x1, blocking collectives, body(): lax.all_to_all(answer, 'ep', 0, 0, tiled=True, axis_index_groups=classes)  20 us
    all_to_all x1, starting transfers between devices, body(): lax.all_to_all(copies, 'ep', 0, 0, tiled=True, axis_index_groups=classes)  10.6 us
    pallas_call x1, Pallas kernels, attend(): pl.pallas_call(functools.partial(attend_kernel, block=block), grid_spec=p...  8.34 us
    pallas_call x7, Pallas kernels, near_call(): pl.pallas_call(kernel, in_specs=[here] * len(arrays), out_specs=[here] *...  5.98 us
    ppermute x1, waiting for transfers between devices, body(): back = lax.ppermute(merge(keep, other), 'ep', pair)  5.49 us
    ppermute x1, waiting for transfers between devices, body(): pair_rows = lax.ppermute(near_rows, 'ep', pair)  5.31 us
  transfers between devices with their start and end apart: 18, of which 9 were waited for; matrix products, arithmetic and copies ran while one was open for 0% of the time, Pallas kernels for 3%

profile of v3, /device:TPU:0, one launch (start us, length us, event | category | flops | bytes accessed | tf_op | source)
XLA Modules:
  0.0 139.5 jit_solution(12205634379280589559)
XLA Ops:
  0.6 0.0 copy-start.11
  0.7 8.3 %attend.1 = (bf16[24,2048]{1,0:T(8,128)(2,1)}, bf16[24,64]{1,0:T(8,128)(2,1)}, bf16[24,64]{1,0:T(8,128)(2,1)}, f32[24,8]{1,0:T(8,128)}) custom-call(s32[24]{0:T(128)} %len_ref.1, f32[1,16]{1,0:T(1,128)} %bitcast.21, bf16[1,64]{1,0:T(2,128)(2,1)} %bitcast.22, bf16[1,64]{1,0:T(2,128)(2,1)} %bitcast.23, bf16[24,2048]{1,0:T(8,128)(2,1)} %tok.1, ...), custom_call_target="tpu_custom_call" | custom-call | tf_op jit(solution)/shard_map/attend/pallas_call | solution.py:193
  9.0 0.0 copy-start.2
  9.0 0.0 copy-start.3
  9.1 0.1 collective-permute-start
  9.2 0.2 shard_map.255.info
  9.3 1.3 collective-permute-done.theirs
  10.6 0.0 copy-done.6
  10.6 0.0 copy-done.9
  10.7 0.9 copy-done.7
  11.5 1.5 %shard_map.256 = (bf16[32,24,1152]{2,1,0:T(8,128)(2,1)}, bf16[24,1024]{1,0:T(8,128)(2,1)S(1)}, f32[24,128]{1,0:T(8,128)S(1)}) custom-call(bf16[24,2048]{1,0:T(8,128)(2,1)S(1)} %copy-done.6, bf16[24,2048]{1,0:T(8,128)(2,1)S(1)} %copy-done.7, bf16[24,2048]{1,0:T(8,128)(2,1)S(1)} %collective-permute-done.theirs, bf16[16,128]{1,0:T(8,128)(2,1)S(1)} %bitcast.15, ...), custom_call_target="tpu_custom_call" | custom-call | tf_op jit(solution)/shard_map/pallas_call | solution.py:57
  13.1 10.6 %all-to-all-start = ((bf16[32,24,1152]{2,1,0:T(8,128)(2,1)}), bf16[32,24,1152]{2,1,0:T(8,128)(2,1)S(1)}, u32[]{:S(2)}, u32[]{:S(2)}) async-start(bf16[32,24,1152]{2,1,0:T(8,128)(2,1)} %get-tuple-element.18), calls=%async_computation | async-start | bytes 3538944 | tf_op jit(solution)/shard_map/all_to_all | solution.py:575
  23.7 0.0 copy-done.2
  23.7 0.3 collective-permute-start.6
  24.0 1.8 %collective-permute-start.8 = (bf16[2048,128]{1,0:T(8,128)(2,1)S(1)}, bf16[2048,128]{1,0:T(8,128)(2,1)S(1)}, u32[]{:S(2)}, u32[]{:S(2)}) collective-permute-start(bf16[2048,128]{1,0:T(8,128)(2,1)S(1)} %copy-done.3), channel_id=1, source_target_pairs={{0,2},{2,0},{4,6},{6,4},{8,10},{10,8},{12,14},{14,12},{16,18},{18,... | collective-permute-start | bytes 1572872 | tf_op jit(solution)/shard_map/ppermute | solution.py:563
  25.8 0.0 collective-permute-start.4
  25.8 0.5 collective-permute-start.5
  26.3 12.3 %collective-permute-done.6.refs_0_ = bf16[2048,128]{1,0:T(8,128)(2,1)S(1)} collective-permute-done((bf16[2048,128]{1,0:T(8,128)(2,1)S(1)}, bf16[2048,128]{1,0:T(8,128)(2,1)S(1)}, u32[]{:S(2)}, u32[]{:S(2)}) %collective-permute-start.6) | collective-permute-done | bytes 524320 | tf_op jit(solution)/shard_map/ppermute | solution.py:563
  38.6 0.0 collective-permute-start.7
  38.6 10.1 %collective-permute-done.8.refs_2_ = bf16[2048,128]{1,0:T(8,128)(2,1)S(1)} collective-permute-done((bf16[2048,128]{1,0:T(8,128)(2,1)S(1)}, bf16[2048,128]{1,0:T(8,128)(2,1)S(1)}, u32[]{:S(2)}, u32[]{:S(2)}) %collective-permute-start.8) | collective-permute-done | bytes 524320 | tf_op jit(solution)/shard_map/ppermute | solution.py:563
  48.7 0.0 collective-permute-start.9
  48.7 0.0 collective-permute-done.4.refs_1_
  48.8 0.0 collective-permute-done.5.refs_3_
  48.8 0.0 copy-start.4
  48.8 1.0 copy-done.4
  49.8 0.2 shard_map.258.own
  50.0 0.0 collective-permute-done.7.refs_1_
  50.0 0.6 collective-permute-done.9.refs_3_
  50.7 0.2 shard_map.259.far
  50.9 0.0 copy-start
  50.9 1.0 copy-done
  51.9 0.0 all-to-all-done
  51.9 1.2 copy-done.1
  53.1 1.8 %shard_map.260.mine = bf16[768,1024]{1,0:T(8,128)(2,1)S(1)} custom-call(bf16[768,1152]{1,0:T(8,128)(2,1)S(1)} %bitcast.13, bf16[1024,512]{1,0:T(8,128)(2,1)S(1)} %shard_map.258.own, bf16[1024,512]{1,0:T(8,128)(2,1)S(1)} %copy-done.1), custom_call_target="tpu_custom_call" | custom-call | tf_op jit(solution)/shard_map/pallas_call | solution.py:57
  54.9 0.2 collective-permute-start.10
  55.1 0.3 collective-permute-start.12
  55.4 0.1 collective-permute-start.11
  55.5 13.8 %collective-permute-done.12.refs_2_ = bf16[128,2048]{1,0:T(8,128)(2,1)S(1)} collective-permute-done((bf16[128,2048]{1,0:T(8,128)(2,1)S(1)}, bf16[128,2048]{1,0:T(8,128)(2,1)S(1)}, u32[]{:S(2)}, u32[]{:S(2)}) %collective-permute-start.12) | collective-permute-done | bytes 524320 | tf_op jit(solution)/shard_map/ppermute | solution.py:563
  69.3 0.0 collective-permute-start.13
  69.3 0.6 shard_map.257
  69.9 0.4 collective-permute-start.1
  70.3 0.3 collective-permute-start.2
  70.6 5.3 %collective-permute-done.1.b0 = bf16[64,1024]{1,0:T(8,128)(2,1)S(1)} collective-permute-done((bf16[64,1024]{1,0:T(8,128)(2,1)S(1)}, bf16[64,1024]{1,0:T(8,128)(2,1)S(1)}, u32[]{:S(2)}, u32[]{:S(2)}) %collective-permute-start.1) | collective-permute-done | bytes 131104 | tf_op jit(solution)/shard_map/ppermute | solution.py:592
  75.9 0.0 collective-permute-start.3
  75.9 0.0 collective-permute-done.11.refs_1_
  75.9 0.0 collective-permute-done.13.refs_3_
  75.9 0.1 shard_map.261.down
  76.0 0.0 collective-permute-done.10.theirs
  76.1 2.9 %dense_down.1 = (bf16[768,1024]{1,0:T(8,128)(2,1)}, f32[32,128]{1,0:T(8,128)S(1)}) custom-call(bf16[768,1024]{1,0:T(8,128)(2,1)S(1)} %shard_map.260.mine, bf16[768,1024]{1,0:T(8,128)(2,1)S(1)} %collective-permute-done.10.theirs, bf16[512,1024]{1,0:T(8,128)(2,1)S(1)} %shard_map.261.down), custom_call_target="tpu_custom_call" | custom-call | tf_op jit(solution)/shard_map/dense_down/pallas_call | solution.py:396
  79.0 0.0 collective-permute-done.2.a1
  79.0 0.0 collective-permute-done.3.b1
  79.0 3.4 %experts.1 = (bf16[128,1024]{1,0:T(8,128)(2,1)S(1)}, bf16[128,1024]{1,0:T(8,128)(2,1)S(1)}) custom-call(bf16[64,1024]{1,0:T(8,128)(2,1)S(1)} %get-tuple-element.19.a0, bf16[64,1024]{1,0:T(8,128)(2,1)S(1)} %collective-permute-done.1.b0, bf16[64,1024]{1,0:T(8,128)(2,1)S(1)} %collective-permute-done.2.a1, bf16[64,1024]{1,0:T(8,128)(2,1)S(1)} %collective-permute-done.3.b1, ...), custom_call_target="tpu_custom_call" | custom-call | tf_op jit(solution)/shard_map/experts/pallas_call | solution.py:447
  82.5 0.6 collective-permute-start.14
  83.0 1.2 collective-permute-done.14.other
  84.2 0.4 collective-permute-start.15
  84.6 5.5 %collective-permute-done.15.near = bf16[64,1024]{1,0:T(8,128)(2,1)S(1)} collective-permute-done((bf16[64,1024]{1,0:T(8,128)(2,1)S(1)}, bf16[64,1024]{1,0:T(8,128)(2,1)S(1)}, u32[]{:S(2)}, u32[]{:S(2)}) %collective-permute-start.15) | collective-permute-done | bytes 131104 | tf_op jit(solution)/shard_map/ppermute | solution.py:603
  90.1 0.6 shard_map.263
  90.7 0.0 copy-start.12
  90.7 0.0 copy-start.10
  90.7 20.0 %all_to_all.15.returned = bf16[32,40,128]{2,1,0:T(8,128)(2,1)S(1)} all-to-all(bf16[32,40,128]{2,1,0:T(8,128)(2,1)S(1)} %shard_map.263), channel_id=1, replica_groups={{0,6,8,14,16,22,24,30,32,38,40,46,48,54,56,62,64,70,72,78,80,86,88,94,9..., dimensions={0} | all-to-all | bytes 655360 | tf_op jit(solution)/shard_map/all_to_all | solution.py:605
  110.7 4.0 %all-to-all-start.2 = ((bf16[32,24,1024]{2,1,0:T(8,128)(2,1)}), bf16[32,24,1024]{2,1,0:T(8,128)(2,1)S(1)}, u32[]{:S(2)}, u32[]{:S(2)}) async-start(bf16[32,24,1024]{2,1,0:T(8,128)(2,1)} %bitcast.9), calls=%async_computation.2 | async-start | bytes 3145728 | tf_op jit(solution)/shard_map/all_to_all | solution.py:594
  114.7 0.7 copy.28
  115.4 22.8 %all-to-all-done.2.parts = bf16[32,24,1024]{2,1,0:T(8,128)(2,1)S(1)} async-done(((bf16[32,24,1024]{2,1,0:T(8,128)(2,1)}), bf16[32,24,1024]{2,1,0:T(8,128)(2,1)S(1)}, u32[]{:S(2)}, u32[]{:S(2)}) %all-to-all-start.2) | async-done | bytes 1572896 | tf_op jit(solution)/shard_map/all_to_all | solution.py:594
  138.2 1.3 shard_map.264
  (13 shorter events, 0.1 us)
Async XLA Ops:
  0.6 8.5 %copy-start.11 = (s32[24,2]{0,1:T(2,128)S(1)}, s32[24,2]{0,1:T(2,128)}, u32[]{:S(2)}) copy-start(s32[24,2]{0,1:T(2,128)} %param.43) | copy-start | bytes 580
  0.6 10.0 %copy-start.6 = (bf16[24,2048]{1,0:T(8,128)(2,1)S(1)}, bf16[24,2048]{1,0:T(8,128)(2,1)}, u32[]{:S(2)}) copy-start(bf16[24,2048]{1,0:T(8,128)(2,1)} %tok.1) | copy-start | bytes 294916
  0.7 10.0 %copy-start.8 = (bf16[2048]{0:T(1024)(128)(2,1)S(1)}, bf16[2048]{0:T(1024)(128)(2,1)}, u32[]{:S(2)}) copy-start(bf16[2048]{0:T(1024)(128)(2,1)} %param.38) | copy-start | bytes 12292
  0.7 10.0 %copy-start.9 = (bf16[2048]{0:T(1024)(128)(2,1)S(1)}, bf16[2048]{0:T(1024)(128)(2,1)}, u32[]{:S(2)}) copy-start(bf16[2048]{0:T(1024)(128)(2,1)} %param.39) | copy-start | bytes 12292
  9.0 14.7 %copy-start.2 = (bf16[2048,128]{1,0:T(8,128)(2,1)S(1)}, bf16[2048,128]{1,0:T(8,128)(2,1)}, u32[]{:S(2)}) copy-start(bf16[2048,128]{1,0:T(8,128)(2,1)} %refs_0_.2) | copy-start | bytes 1572868
  9.0 15.0 %copy-start.3 = (bf16[2048,128]{1,0:T(8,128)(2,1)S(1)}, bf16[2048,128]{1,0:T(8,128)(2,1)}, u32[]{:S(2)}) copy-start(bf16[2048,128]{1,0:T(8,128)(2,1)} %refs_2_.1) | copy-start | bytes 1572868
  9.1 1.6 %collective-permute-start = (bf16[24,2048]{1,0:T(8,128)(2,1)}, bf16[24,2048]{1,0:T(8,128)(2,1)S(1)}, u32[]{:S(2)}, u32[]{:S(2)}) collective-permute-start(bf16[24,2048]{1,0:T(8,128)(2,1)} %get-tuple-element.17.mine), channel_id=1, source_target_pairs={{0,1},{1,0},{2,3},{3,2},{4,5},{5,4},{6,7},{7,6},{8,9},{9,8},{10,11... | collective-permute-start | bytes 294920 | tf_op jit(solution)/shard_map/ppermute | solution.py:27
  10.7 0.9 copy-start.7
  13.1 38.8 %all-to-all-start = ((bf16[32,24,1152]{2,1,0:T(8,128)(2,1)}), bf16[32,24,1152]{2,1,0:T(8,128)(2,1)S(1)}, u32[]{:S(2)}, u32[]{:S(2)}) async-start(bf16[32,24,1152]{2,1,0:T(8,128)(2,1)} %get-tuple-element.18), calls=%async_computation | async-start | bytes 3538944 | tf_op jit(solution)/shard_map/all_to_all | solution.py:575
  23.7 14.9 %collective-permute-start.6 = (bf16[2048,128]{1,0:T(8,128)(2,1)S(1)}, bf16[2048,128]{1,0:T(8,128)(2,1)S(1)}, u32[]{:S(2)}, u32[]{:S(2)}) collective-permute-start(bf16[2048,128]{1,0:T(8,128)(2,1)S(1)} %copy-done.2), channel_id=1, source_target_pairs={{0,2},{2,0},{4,6},{6,4},{8,10},{10,8},{12,14},{14,12},{16,18},{18,... | collective-permute-start | bytes 1572872 | tf_op jit(solution)/shard_map/ppermute | solution.py:563
  24.0 24.7 %collective-permute-start.8 = (bf16[2048,128]{1,0:T(8,128)(2,1)S(1)}, bf16[2048,128]{1,0:T(8,128)(2,1)S(1)}, u32[]{:S(2)}, u32[]{:S(2)}) collective-permute-start(bf16[2048,128]{1,0:T(8,128)(2,1)S(1)} %copy-done.3), channel_id=1, source_target_pairs={{0,2},{2,0},{4,6},{6,4},{8,10},{10,8},{12,14},{14,12},{16,18},{18,... | collective-permute-start | bytes 1572872 | tf_op jit(solution)/shard_map/ppermute | solution.py:563
  25.8 22.9 %collective-permute-start.4 = (bf16[2048,128]{1,0:T(8,128)(2,1)S(1)}, bf16[2048,128]{1,0:T(8,128)(2,1)S(1)}, u32[]{:S(2)}, u32[]{:S(2)}) collective-permute-start(bf16[2048,128]{1,0:T(8,128)(2,1)S(1)} %copy-done.2), channel_id=1, source_target_pairs={{0,1},{1,0},{2,3},{3,2},{4,5},{5,4},{6,7},{7,6},{8,9},{9,8},{10,11... | collective-permute-start | bytes 1572872 | tf_op jit(solution)/shard_map/ppermute | solution.py:27
  25.8 22.9 %collective-permute-start.5 = (bf16[2048,128]{1,0:T(8,128)(2,1)S(1)}, bf16[2048,128]{1,0:T(8,128)(2,1)S(1)}, u32[]{:S(2)}, u32[]{:S(2)}) collective-permute-start(bf16[2048,128]{1,0:T(8,128)(2,1)S(1)} %copy-done.3), channel_id=1, source_target_pairs={{0,1},{1,0},{2,3},{3,2},{4,5},{5,4},{6,7},{7,6},{8,9},{9,8},{10,11... | collective-permute-start | bytes 1572872 | tf_op jit(solution)/shard_map/ppermute | solution.py:27
  38.6 11.4 %collective-permute-start.7 = (bf16[2048,128]{1,0:T(8,128)(2,1)S(1)}, bf16[2048,128]{1,0:T(8,128)(2,1)S(1)}, u32[]{:S(2)}, u32[]{:S(2)}) collective-permute-start(bf16[2048,128]{1,0:T(8,128)(2,1)S(1)} %collective-permute-done.6.refs_0_), channel_id=1, source_target_pairs={{0,1},{1,0},{2,3},{3,2},{4,5},{5,4},{6,7},{7,6},{8,9},{9,8},{10,11... | collective-permute-start | bytes 1572872 | tf_op jit(solution)/shard_map/ppermute | solution.py:27
  48.7 1.9 %collective-permute-start.9 = (bf16[2048,128]{1,0:T(8,128)(2,1)S(1)}, bf16[2048,128]{1,0:T(8,128)(2,1)S(1)}, u32[]{:S(2)}, u32[]{:S(2)}) collective-permute-start(bf16[2048,128]{1,0:T(8,128)(2,1)S(1)} %collective-permute-done.8.refs_2_), channel_id=1, source_target_pairs={{0,1},{1,0},{2,3},{3,2},{4,5},{5,4},{6,7},{7,6},{8,9},{9,8},{10,11... | collective-permute-start | bytes 1572872 | tf_op jit(solution)/shard_map/ppermute | solution.py:27
  48.8 1.0 copy-start.4
  50.9 1.0 copy-start
  51.9 1.2 copy-start.1
  53.1 2.0 %copy-start.5 = (bf16[128,2048]{1,0:T(8,128)(2,1)S(1)}, bf16[128,2048]{1,0:T(8,128)(2,1)}, u32[]{:S(2)}) copy-start(bf16[128,2048]{1,0:T(8,128)(2,1)} %refs_0_.3) | copy-start | bytes 1572868
  54.9 21.2 %collective-permute-start.10 = (bf16[768,1024]{1,0:T(8,128)(2,1)S(1)}, bf16[768,1024]{1,0:T(8,128)(2,1)S(1)}, u32[]{:S(2)}, u32[]{:S(2)}) collective-permute-start(bf16[768,1024]{1,0:T(8,128)(2,1)S(1)} %shard_map.260.mine), channel_id=1, source_target_pairs={{0,1},{1,0},{2,3},{3,2},{4,5},{5,4},{6,7},{7,6},{8,9},{9,8},{10,11... | collective-permute-start | bytes 4718600 | tf_op jit(solution)/shard_map/ppermute | solution.py:27
  55.1 14.2 %collective-permute-start.12 = (bf16[128,2048]{1,0:T(8,128)(2,1)S(1)}, bf16[128,2048]{1,0:T(8,128)(2,1)S(1)}, u32[]{:S(2)}, u32[]{:S(2)}) collective-permute-start(bf16[128,2048]{1,0:T(8,128)(2,1)S(1)} %copy-done.5), channel_id=1, source_target_pairs={{0,2},{2,0},{4,6},{6,4},{8,10},{10,8},{12,14},{14,12},{16,18},{18,... | collective-permute-start | bytes 1572872 | tf_op jit(solution)/shard_map/ppermute | solution.py:563
  55.4 20.5 %collective-permute-start.11 = (bf16[128,2048]{1,0:T(8,128)(2,1)S(1)}, bf16[128,2048]{1,0:T(8,128)(2,1)S(1)}, u32[]{:S(2)}, u32[]{:S(2)}) collective-permute-start(bf16[128,2048]{1,0:T(8,128)(2,1)S(1)} %copy-done.5), channel_id=1, source_target_pairs={{0,1},{1,0},{2,3},{3,2},{4,5},{5,4},{6,7},{7,6},{8,9},{9,8},{10,11... | collective-permute-start | bytes 1572872 | tf_op jit(solution)/shard_map/ppermute | solution.py:27
  69.3 6.6 %collective-permute-start.13 = (bf16[128,2048]{1,0:T(8,128)(2,1)S(1)}, bf16[128,2048]{1,0:T(8,128)(2,1)S(1)}, u32[]{:S(2)}, u32[]{:S(2)}) collective-permute-start(bf16[128,2048]{1,0:T(8,128)(2,1)S(1)} %collective-permute-done.12.refs_2_), channel_id=1, source_target_pairs={{0,1},{1,0},{2,3},{3,2},{4,5},{5,4},{6,7},{7,6},{8,9},{9,8},{10,11... | collective-permute-start | bytes 1572872 | tf_op jit(solution)/shard_map/ppermute | solution.py:27
  69.9 6.0 %collective-permute-start.1 = (bf16[64,1024]{1,0:T(8,128)(2,1)S(1)}, bf16[64,1024]{1,0:T(8,128)(2,1)S(1)}, u32[]{:S(2)}, u32[]{:S(2)}) collective-permute-start(bf16[64,1024]{1,0:T(8,128)(2,1)S(1)} %get-tuple-element.20), channel_id=1, source_target_pairs={{0,2},{2,0},{4,6},{6,4},{8,10},{10,8},{12,14},{14,12},{16,18},{18,... | collective-permute-start | bytes 393224 | tf_op jit(solution)/shard_map/ppermute | solution.py:592
  70.3 8.7 %collective-permute-start.2 = (bf16[64,1024]{1,0:T(8,128)(2,1)S(1)}, bf16[64,1024]{1,0:T(8,128)(2,1)S(1)}, u32[]{:S(2)}, u32[]{:S(2)}) collective-permute-start(bf16[64,1024]{1,0:T(8,128)(2,1)S(1)} %get-tuple-element.19.a0), channel_id=1, source_target_pairs={{0,1},{1,0},{2,3},{3,2},{4,5},{5,4},{6,7},{7,6},{8,9},{9,8},{10,11... | collective-permute-start | bytes 393224 | tf_op jit(solution)/shard_map/ppermute | solution.py:27
  75.9 3.1 %collective-permute-start.3 = (bf16[64,1024]{1,0:T(8,128)(2,1)S(1)}, bf16[64,1024]{1,0:T(8,128)(2,1)S(1)}, u32[]{:S(2)}, u32[]{:S(2)}) collective-permute-start(bf16[64,1024]{1,0:T(8,128)(2,1)S(1)} %collective-permute-done.1.b0), channel_id=1, source_target_pairs={{0,1},{1,0},{2,3},{3,2},{4,5},{5,4},{6,7},{7,6},{8,9},{9,8},{10,11... | collective-permute-start | bytes 393224 | tf_op jit(solution)/shard_map/ppermute | solution.py:27
  82.5 1.7 %collective-permute-start.14 = (bf16[128,1024]{1,0:T(8,128)(2,1)S(1)}, bf16[128,1024]{1,0:T(8,128)(2,1)S(1)}, u32[]{:S(2)}, u32[]{:S(2)}) collective-permute-start(bf16[128,1024]{1,0:T(8,128)(2,1)S(1)} %get-tuple-element.23), channel_id=1, source_target_pairs={{0,1},{1,0},{2,3},{3,2},{4,5},{5,4},{6,7},{7,6},{8,9},{9,8},{10,11... | collective-permute-start | bytes 786440 | tf_op jit(solution)/shard_map/ppermute | solution.py:27
  84.2 5.9 %collective-permute-start.15 = (bf16[64,1024]{1,0:T(8,128)(2,1)S(1)}, bf16[64,1024]{1,0:T(8,128)(2,1)S(1)}, u32[]{:S(2)}, u32[]{:S(2)}) collective-permute-start(bf16[64,1024]{1,0:T(8,128)(2,1)S(1)} %shard_map.262), channel_id=1, source_target_pairs={{0,2},{2,0},{4,6},{6,4},{8,10},{10,8},{12,14},{14,12},{16,18},{18,... | collective-permute-start | bytes 393224 | tf_op jit(solution)/shard_map/ppermute | solution.py:603
  90.7 24.0 %copy-start.12 = (f32[24,8]{1,0:T(8,128)S(1)}, f32[24,8]{1,0:T(8,128)}, u32[]{:S(2)}) copy-start(f32[24,8]{1,0:T(8,128)} %get-tuple-element.33) | copy-start | bytes 2308
  90.7 47.5 %copy-start.10 = (f32[24,2]{0,1:T(2,128)S(1)}, f32[24,2]{0,1:T(2,128)}, u32[]{:S(2)}) copy-start(f32[24,2]{0,1:T(2,128)} %param.44) | copy-start | bytes 580
  110.7 27.5 %all-to-all-start.2 = ((bf16[32,24,1024]{2,1,0:T(8,128)(2,1)}), bf16[32,24,1024]{2,1,0:T(8,128)(2,1)S(1)}, u32[]{:S(2)}, u32[]{:S(2)}) async-start(bf16[32,24,1024]{2,1,0:T(8,128)(2,1)} %bitcast.9), calls=%async_computation.2 | async-start | bytes 3145728 | tf_op jit(solution)/shard_map/all_to_all | solution.py:594
